TPU v7x, 32 devices: a whole 2x2x4 slice. The times are simulated.
32 devices in a mesh: sp: 8 (over z, y), tp: 4 (over x, core).
Axes of the slice: x: 2, y: 2, z: 4, core: 2. Of those that a mesh axis runs over, the one named last changes fastest.
Arguments:
- expert_in: bfloat16 [1024, 2048], P('sp'), may hold values from -6 to 6
- out_cot: bfloat16 [1024, 2048], P('sp'), may hold values from -8 to 8
- route_ids: int32 [1024, 2], P('sp'), may hold values from 0 to 7, all different within a row; in each aligned block of 128 rows (0 to 127, 128 to 255, ...) at most 64 rows name the same one
- route_weights: float32 [1024, 2], P('sp'), may hold values from 0.1 to 1
- w_gate: bfloat16 [8, 2048, 1024], P('sp', None, 'tp'), may hold values from -0.125 to 0.125
- w_up: bfloat16 [8, 2048, 1024], P('sp', None, 'tp'), may hold values from -0.125 to 0.125
- w_down: bfloat16 [8, 1024, 2048], P('sp', 'tp'), may hold values from -0.1875 to 0.1875
- w_out: bfloat16 [2048, 1024], P(None, 'tp'), may hold values from -0.1875 to 0.1875
- mixed_heads: bfloat16 [1024, 1024], P('sp', 'tp'), may hold values from -6 to 6
- queries: bfloat16 [1024, 512], P('sp', 'tp'), may hold values from -0.5 to 0.5
- keys: bfloat16 [1024, 512], P('sp', 'tp'), may hold values from -0.3125 to 0.3125
- values: bfloat16 [1024, 1024], P('sp', 'tp'), may hold values from -6 to 6
- log_decay: float32 [1024, 512], P('sp', 'tp'), may hold values from -0.3 to 0
Outputs:
- grad_gate: float32 [8, 2048, 1024], P('sp', None, 'tp')
- grad_up: float32 [8, 2048, 1024], P('sp', None, 'tp')
- grad_down: float32 [8, 1024, 2048], P('sp', 'tp')
- grad_out_proj: float32 [2048, 1024], P('sp', 'tp')
- grad_queries: bfloat16 [1024, 512], P('sp', 'tp')
- grad_keys: bfloat16 [1024, 512], P('sp', 'tp')
- grad_values: bfloat16 [1024, 1024], P('sp', 'tp')
- grad_decay: float32 [1024, 512], P('sp', 'tp')
Inputs may be any that keep to these rules, and one draw needn't show every extreme that they name: `route_ids`: in the rows of one device no expert is named more than 64 times, a bound that some block reaches.
All inputs are finite; a program needn't handle non-finite values.
Results may differ from a plain program's by a relative error of at most 0.015.
Values may be sent and summed in bfloat16 or wider, within the bound.
A program may use at most 128 MiB of HBM per device.

v0:
```python
import functools

import jax
import jax.numpy as jnp
from jax import lax
from jax.experimental import pallas as pl
from jax.experimental.pallas import tpu as pltpu
from jax.sharding import PartitionSpec as P

DK = 128
EXACT = lax.Precision.HIGHEST
MESH = pl.DeviceIdType.MESH


def remote(src, dst, send, recv, device):
    return pltpu.make_async_remote_copy(
        src_ref=src, dst_ref=dst, send_sem=send, recv_sem=recv, device_id=device, device_id_type=MESH
    )


def greet(n_sp, me, tp, partners):
    barrier = pltpu.get_barrier_semaphore()

    def hello(i, carry):
        pl.semaphore_signal(
            barrier, inc=1, device_id=(lax.rem(me + i, n_sp), tp), device_id_type=MESH
        )
        return carry

    lax.fori_loop(1, n_sp, hello, 0)
    for other in partners:
        pl.semaphore_signal(barrier, inc=1, device_id=(me, other), device_id_type=MESH)
    pl.semaphore_wait(barrier, n_sp - 1 + len(partners))


def loop(start, stop, body):
    def step(i, carry):
        body(i)
        return carry

    lax.fori_loop(start, stop, step, 0)


def spread_kernel(n_sp, n_tp, n_rows, n_sides, *refs):
    count = n_rows + n_sides
    given, got = refs[:count], refs[count : 2 * count]
    s0, r0, s1, r1, s2, r2, s3, r3, s4, r4, own_sem = refs[2 * count :]
    me, tp = lax.axis_index("sp"), lax.axis_index("tp")
    far = lax.rem(tp + n_tp // 2, n_tp)
    near = tp + 1 - 2 * lax.rem(tp, 2)
    greet(n_sp, me, tp, (far, near))
    rows = tuple(zip(given[:n_rows], got[:n_rows]))
    sides = tuple(zip(given[n_rows:], got[n_rows:]))

    def first(j, p, slot):
        return remote(rows[j][0].at[p], rows[j][1].at[slot, tp], s0.at[j, p], r0.at[j, slot], (p, tp))

    def across(j, p, share):
        ref = rows[j][1].at[p, share]
        return remote(ref, ref, s1.at[j, p], r1.at[j, p], (me, far))

    def beside(j, p, share):
        ref = rows[j][1].at[p, share]
        return remote(ref, ref, s2.at[j, p], r2.at[j, p], (me, near))

    def relay(j, p, share):
        ref = rows[j][1].at[p, share]
        return remote(ref, ref, s3.at[j, p], r3.at[j, p], (me, near))

    def side(k, p, slot):
        return remote(sides[k][0], sides[k][1].at[slot], s4.at[k, p], r4.at[k, slot], (p, tp))

    def send(i):
        p = lax.rem(me + i, n_sp)
        for j in range(n_rows):
            first(j, p, me).start()

    loop(1, n_sp, send)
    owns = [
        pltpu.make_async_copy(rows[j][0].at[me], rows[j][1].at[me, tp], own_sem.at[j]) for j in range(n_rows)
    ] + [pltpu.make_async_copy(sides[k][0], sides[k][1].at[me], own_sem.at[n_rows + k]) for k in range(n_sides)]
    for own in owns:
        own.start()
    for own in owns:
        own.wait()
    for j in range(n_rows):
        across(j, me, tp).start()
        beside(j, me, tp).start()

    def send_side(i):
        p = lax.rem(me + i, n_sp)
        for k in range(n_sides):
            side(k, p, me).start()

    loop(1, n_sp, send_side)

    def forward(i):
        p = lax.rem(me - i + n_sp, n_sp)
        for j in range(n_rows):
            first(j, p, p).wait_recv()
            across(j, p, tp).start()
            beside(j, p, tp).start()

    loop(1, n_sp, forward)

    def pass_on(i):
        p = lax.rem(me - i + n_sp, n_sp)
        for j in range(n_rows):
            across(j, p, far).wait_recv()
            relay(j, p, far).start()

    loop(0, n_sp, pass_on)
    near_far = lax.rem(near + n_tp // 2, n_tp)

    def finish(i):
        p = lax.rem(me - i + n_sp, n_sp)
        for j in range(n_rows):
            beside(j, p, near).wait_recv()
            relay(j, p, near_far).wait_recv()
            across(j, p, tp).wait_send()
            beside(j, p, tp).wait_send()
            relay(j, p, far).wait_send()

    loop(0, n_sp, finish)

    def finish_side(i):
        p = lax.rem(me - i + n_sp, n_sp)
        for k in range(n_sides):
            side(k, p, p).wait_recv()
            side(k, p, me).wait_send()
        for j in range(n_rows):
            first(j, p, me).wait_send()

    loop(1, n_sp, finish_side)


def return_kernel(
    n_sp, n_tp, part, comb, dy, mix, state, mid, gmix, gstate, in1, out1, in2, out2, ret,
    s1, r1, s2, r2, s3, r3, s4, r4, s5, r5, own_sem,
):
    me, tp = lax.axis_index("sp"), lax.axis_index("tp")
    far = lax.rem(tp + n_tp // 2, n_tp)
    near = tp + 1 - 2 * lax.rem(tp, 2)
    near_far = lax.rem(near + n_tp // 2, n_tp)
    quarter = part.shape[2] // n_tp
    greet(n_sp, me, tp, (far, near))

    gathered = ((mix, gmix), (state, gstate))
    strides = [n_sp >> (k + 1) for k in range(n_sp.bit_length() - 1)]

    def hop(j, k, base, c):
        block = lax.rem(base, 2 * strides[k]) + c * 2 * strides[k]
        partner = me + strides[k] * (1 - 2 * lax.rem(me // strides[k], 2))
        ref = gathered[j][1].at[block]
        return remote(ref, ref, s5.at[j, k, c], r5.at[j, block], (partner, tp))

    def widen(k):
        def one(c):
            for j in (0, 1):
                hop(j, k, me, c).start()

        loop(0, n_sp // (2 * strides[k]), one)

    def arrive(k):
        partner = me + strides[k] * (1 - 2 * lax.rem(me // strides[k], 2))

        def one(c):
            for j in (0, 1):
                hop(j, k, partner, c).wait_recv()
                hop(j, k, me, c).wait_send()

        loop(0, n_sp // (2 * strides[k]), one)

    def columns(block):
        return pl.ds(pl.multiple_of(block * quarter, quarter), quarter)

    def beside(j, p):
        block = near if j == 0 else near_far
        return remote(
            part.at[p, :, columns(block)], in1.at[p, j], s1.at[j, p], r1.at[j, p], (me, near)
        )

    def across(p):
        return remote(out1.at[p], in2.at[p], s2.at[p], r2.at[p], (me, far))

    def back(p, slot):
        return remote(out2.at[p], ret.at[slot], s3.at[p], r3.at[slot], (p, tp))

    def start(i):
        p = lax.rem(me + 1 + i, n_sp)
        for j in (1, 0):
            beside(j, p).start()

    loop(0, n_sp, start)
    owns = [
        pltpu.make_async_copy(gathered[j][0], gathered[j][1].at[me], own_sem.at[j]) for j in (0, 1)
    ]
    for own in owns:
        own.start()
    for own in owns:
        own.wait()
    widen(0)

    def pair(i):
        p = lax.rem(me + 1 + i, n_sp)
        beside(1, p).wait_recv()
        mine = part[p, :, columns(far)].astype(jnp.float32)
        out1[p] = (mine + in1[p, 1].astype(jnp.float32)).astype(jnp.bfloat16)
        across(p).start()

    loop(0, n_sp, pair)
    arrive(0)
    for k in range(1, len(strides) - 1):
        widen(k)
        arrive(k)

    def total(p):
        beside(0, p).wait_recv()
        across(p).wait_recv()
        mine = part[p, :, columns(tp)].astype(jnp.float32)
        mine = mine + in1[p, 0].astype(jnp.float32)
        return (mine + in2[p].astype(jnp.float32)).astype(jnp.bfloat16)

    def quad(i):
        p = lax.rem(me + i, n_sp)
        out2[p] = total(p)
        back(p, me).start()

    loop(1, n_sp, quad)
    ret[me] = total(me)
    widen(len(strides) - 1)

    def gather(i, acc):
        p = lax.rem(me - i + n_sp, n_sp)

        @pl.when(i > 0)
        def _():
            back(p, p).wait_recv()

        return acc + jnp.dot(comb[p], ret[p], preferred_element_type=jnp.float32)

    acc = lax.fori_loop(0, n_sp, gather, dy[:, columns(tp)].astype(jnp.float32))
    mid[:, columns(tp)] = acc.astype(jnp.bfloat16)

    def share(k, block, device):
        ref = mid.at[:, columns(block)]
        return remote(ref, ref, s4.at[k], r4.at[k], (me, device))

    share(0, tp, far).start()
    share(1, tp, near).start()
    share(0, far, far).wait_recv()
    share(2, far, near).start()
    share(1, near, near).wait_recv()
    share(2, near_far, near).wait_recv()
    share(0, tp, far).wait_send()
    share(1, tp, near).wait_send()
    share(2, far, near).wait_send()

    arrive(len(strides) - 1)

    def finish(i):
        p = lax.rem(me + i, n_sp)
        for j in (0, 1):
            beside(j, p).wait_send()
        across(p).wait_send()

        @pl.when(i > 0)
        def _():
            back(p, me).wait_send()

    loop(0, n_sp, finish)


VM = pl.BlockSpec(memory_space=pltpu.VMEM)
ANY = pl.BlockSpec(memory_space=pl.ANY)


def dma(*shape):
    return [pltpu.SemaphoreType.DMA(shape), pltpu.SemaphoreType.DMA(shape)]


def call(kernel, ident, operands, in_specs, out_shape, out_specs, scratch):
    return pl.pallas_call(
        kernel,
        out_shape=out_shape,
        in_specs=in_specs,
        out_specs=out_specs,
        scratch_shapes=scratch,
        compiler_params=pltpu.CompilerParams(
            collective_id=ident, has_side_effects=True, vmem_limit_bytes=48 * 1024 * 1024
        ),
    )(*operands)


def per_device(
    expert_in, out_cot, route_ids, route_weights, w_gate, w_up, w_down, w_out,
    mixed_heads, queries, keys, values, log_decay,
):
    bf16, f32 = jnp.bfloat16, jnp.float32
    n_sp, n_tp = lax.axis_size("sp"), lax.axis_size("tp")
    me, tp = lax.axis_index("sp"), lax.axis_index("tp")
    tok, width = expert_in.shape
    top = route_ids.shape[1]
    experts = w_gate.shape[0] * n_sp
    cap = 2 * top * tok // experts
    share = cap // n_tp

    ids = route_ids.reshape(-1)
    onehot = ids[:, None] == jnp.arange(experts, dtype=jnp.int32)
    order = jnp.arange(tok * top, dtype=jnp.int32)
    below = (order[None, :] < order[:, None]).astype(bf16)
    ranks = jnp.dot(below, onehot.astype(bf16), preferred_element_type=f32)
    rank = jnp.sum(jnp.where(onehot, ranks, 0.0), axis=1).astype(jnp.int32)
    slot = (ids * cap + rank).reshape(tok, top)
    mine = (
        jnp.arange(experts, dtype=jnp.int32)[:, None] * cap
        + tp * share
        + jnp.arange(share, dtype=jnp.int32)[None, :]
    ).reshape(-1)
    match = slot[None] == mine[:, None, None]
    pick = jnp.any(match, axis=2).astype(bf16)
    slot_weight = jnp.sum(jnp.where(match, route_weights[None], 0.0), axis=(1, 2))
    x_share = jnp.dot(pick, expert_in, preferred_element_type=f32).astype(bf16)
    dy_share = (
        slot_weight[:, None] * jnp.dot(pick, out_cot, preferred_element_type=f32)
    ).astype(bf16)
    places = jnp.arange(experts * cap, dtype=jnp.int32).reshape(experts, 1, cap, 1)
    comb = jnp.any(slot[None, :, None, :] == places, axis=3).astype(bf16)

    heads = queries.shape[1] // DK
    dv = values.shape[1] // heads
    step = jnp.arange(tok, dtype=jnp.int32)
    causal = step[None, :] <= step[:, None]
    lower = causal.astype(f32)
    cumulative = jnp.dot(lower, log_decay, precision=EXACT)
    decay_sum = cumulative[-1:]

    def split(array):
        return array.astype(f32).reshape(tok, heads, -1)

    q, k, v = split(queries), split(keys), split(values)
    grow, shrink, to_end = (
        split(jnp.exp(-cumulative)),
        split(jnp.exp(cumulative)),
        split(jnp.exp(decay_sum - cumulative)),
    )
    qd, kg, ke = q * shrink, k * grow, k * to_end
    state_local = jnp.einsum("thd,the->hde", ke, v, precision=EXACT)

    rows = jax.ShapeDtypeStruct((n_sp, n_tp, share, width), bf16)
    gx, gdy, gdecay = call(
        functools.partial(spread_kernel, n_sp, n_tp, 2, 1),
        0,
        (
            x_share.reshape(n_sp, share, width),
            dy_share.reshape(n_sp, share, width),
            decay_sum,
        ),
        [VM] * 3,
        (
            rows,
            rows,
            jax.ShapeDtypeStruct((n_sp,) + decay_sum.shape, f32),
        ),
        (ANY, ANY, ANY),
        dma(2, n_sp) * 4 + dma(1, n_sp) + [pltpu.SemaphoreType.DMA((3,))],
    )
    got_x = gx.reshape(n_sp * cap, width)
    got_dy = gdy.reshape(n_sp * cap, width)
    wg, wu, wd = w_gate[0], w_up[0], w_down[0]
    gate_pre = jnp.dot(got_x, wg, preferred_element_type=f32)
    up_pre = jnp.dot(got_x, wu, preferred_element_type=f32)
    hidden_cot = lax.dot_general(got_dy, wd, (((1,), (1,)), ((), ())), preferred_element_type=f32)
    sig = jax.nn.sigmoid(gate_pre)
    hidden = (gate_pre * sig * up_pre).astype(bf16)
    gate_cot = (hidden_cot * up_pre * sig * (1.0 + gate_pre * (1.0 - sig))).astype(bf16)
    up_cot = (hidden_cot * gate_pre * sig).astype(bf16)
    back = (((1,), (1,)), ((), ()))
    part = lax.dot_general(gate_cot, wg, back, preferred_element_type=f32) + lax.dot_general(
        up_cot, wu, back, preferred_element_type=f32
    )
    part = part.astype(bf16).reshape(n_sp, cap, width)
    over = (((0,), (0,)), ((), ()))
    grad_gate = lax.dot_general(got_x, gate_cot, over, preferred_element_type=f32)[None]
    grad_up = lax.dot_general(got_x, up_cot, over, preferred_element_type=f32)[None]
    grad_down = lax.dot_general(hidden, got_dy, over, preferred_element_type=f32)[None]

    quarter = width // n_tp
    buf = pltpu.VMEM((n_sp, cap, quarter), bf16)
    mid, gmix, gstate = call(
        functools.partial(return_kernel, n_sp, n_tp),
        1,
        (part, comb, out_cot, mixed_heads, state_local.reshape(heads * DK, dv).astype(bf16)),
        [VM] * 5,
        (
            jax.ShapeDtypeStruct((tok, width), bf16),
            jax.ShapeDtypeStruct((n_sp,) + mixed_heads.shape, bf16),
            jax.ShapeDtypeStruct((n_sp, heads * DK, dv), bf16),
        ),
        (VM, VM, VM),
        [pltpu.VMEM((n_sp, 2, cap, quarter), bf16), buf, buf, buf, buf]
        + dma(2, n_sp) + dma(n_sp) + dma(n_sp) + dma(3)
        + [
            pltpu.SemaphoreType.DMA((2, n_sp.bit_length() - 1, n_sp // 2)),
            pltpu.SemaphoreType.DMA((2, n_sp)),
            pltpu.SemaphoreType.DMA((2,)),
        ],
    )
    head_cot = split(jnp.dot(mid, w_out, preferred_element_type=f32))
    pull = jnp.einsum("thd,the->hde", qd, head_cot, precision=EXACT)
    part_tok = tok // n_tp
    cols = lax.dynamic_slice_in_dim(mid, tp * part_tok, part_tok, 0)
    cols = cols.reshape(part_tok, n_sp, width // n_sp).swapaxes(0, 1)
    gcols, gpull = call(
        functools.partial(spread_kernel, n_sp, n_tp, 1, 1),
        2,
        (cols, pull.reshape(heads * DK, dv).astype(bf16)),
        [VM] * 2,
        (
            jax.ShapeDtypeStruct((n_sp, n_tp, part_tok, width // n_sp), bf16),
            jax.ShapeDtypeStruct((n_sp, heads * DK, dv), bf16),
        ),
        (VM, VM),
        dma(1, n_sp) * 5 + [pltpu.SemaphoreType.DMA((2,))],
    )
    gcols = gcols.reshape(n_sp, tok, width // n_sp)
    grad_out_proj = jnp.einsum("ntd,nte->de", gcols, gmix, preferred_element_type=f32)

    sums = gdecay[:, 0]
    index = jnp.arange(n_sp, dtype=jnp.int32)
    between = (index[None] > jnp.minimum(index, me)[:, None]) & (
        index[None] < jnp.maximum(index, me)[:, None]
    )
    weight = jnp.exp(jnp.sum(jnp.where(between[..., None], sums[None], 0.0), axis=1))

    def entering(pieces, used):
        scale = jnp.where(used[:, None], weight, 0.0)
        return jnp.sum(scale[..., None] * pieces.astype(f32), axis=0).reshape(heads, DK, dv)

    state_in = entering(gstate, index < me)
    state_cot = entering(gpull, index > me)

    dot = functools.partial(jnp.einsum, precision=EXACT)
    scores = jnp.where(causal, dot("thd,shd->hts", qd, kg), 0.0)
    scores_cot = jnp.where(causal, dot("the,she->hts", head_cot, v), 0.0)
    grad_v = dot("hts,the->she", scores, head_cot) + dot("shd,hde->she", ke, state_cot)
    qd_cot = dot("hts,shd->thd", scores_cot, kg) + dot("the,hde->thd", head_cot, state_in)
    kg_cot = dot("hts,thd->shd", scores_cot, qd)
    ke_cot = dot("she,hde->shd", v, state_cot)
    end = ke_cot * ke
    c_cot = (qd_cot * qd - kg_cot * kg - end).reshape(tok, heads * DK)
    last = jnp.sum(end, axis=0).reshape(-1) + jnp.exp(decay_sum[0]) * jnp.sum(
        state_cot * state_in, axis=2
    ).reshape(-1)
    grad_decay = lax.dot_general(lower, c_cot, over, precision=EXACT) + last[None]
    grad_q = (qd_cot * shrink).astype(bf16).reshape(tok, heads * DK)
    grad_k = (kg_cot * grow + ke_cot * to_end).astype(bf16).reshape(tok, heads * DK)
    return (
        grad_gate,
        grad_up,
        grad_down,
        grad_out_proj,
        grad_q,
        grad_k,
        grad_v.astype(bf16).reshape(tok, heads * dv),
        grad_decay,
    )


def solution(mesh):
    tokens, both = P("sp", None), P("sp", "tp")
    up, down = P("sp", None, "tp"), P("sp", "tp", None)
    return jax.shard_map(
        per_device,
        mesh=mesh,
        in_specs=(tokens,) * 4 + (up, up, down, P(None, "tp")) + (both,) * 5,
        out_specs=(up, up, down) + (both,) * 5,
        check_vma=False,
    )
```

profile of v0, /device:TPU:0, one launch (start us, length us, event | category | flops | bytes accessed | tf_op | source)
XLA Modules:
  0.0 134.5 jit_solution(5859867283112880006)
XLA Ops:
  0.8 1.0 copy.51
  1.8 0.1 eq.20
  1.9 0.2 fusion.4
  2.4 0.7 multiply_add_fusion.1
  3.2 0.9 fusion.15
  4.0 1.3 fusion
  5.4 1.0 fusion.23
  6.4 1.4 %convolution_convert_fusion = bf16[128,2048]{1,0:T(8,128)(2,1)S(1)} fusion(pred[128,128]{1,0:T(8,128)(4,1)S(1)} %compare_reduce_fusion.1, bf16[128,2048]{1,0:T(8,128)(2,1)} %param.13), kind=kOutput, calls=%fused_computation.6 | convolution fusion | flops 67371008 | bytes 1064960 | tf_op jit(solution)/shard_map/dot_general | solution.py:323
  7.8 38.8 %shard_map.188 = (bf16[8,4,16,2048]{3,2,1,0:T(8,128)(2,1)S(1)}, bf16[8,4,16,2048]{3,2,1,0:T(8,128)(2,1)S(1)}, f32[8,1,128]{2,1,0:T(1,128)S(1)}) custom-call(bf16[8,16,2048]{2,1,0:T(8,128)(2,1)S(1)} %bitcast.150, bf16[8,16,2048]{2,1,0:T(8,128)(2,1)S(1)} %bitcast.151, f32[1,128]{1,0:T(1,128)S(1)} %get-tuple-element.62.refs_2_), custom_call_target="tpu_custom_call" | custom-call | tf_op jit(solution)/shard_map/pallas_call | solution.py:283
  46.6 0.7 fusion.10
  47.4 0.7 fusion.7
  48.1 0.5 copy-done.1
  48.6 0.8 copy-done.28
  49.4 0.8 multiply_convert_fusion.1
  50.3 0.7 fusion.5
  51.0 0.6 copy-done.16
  51.7 0.7 add_convert_fusion
  52.5 0.3 convolution_convert_fusion.2.state
  52.8 0.1 compare_reduce_fusion
  53.0 0.7 convert_element_type.77
  53.6 1.1 copy.53.comb
  54.7 1.0 copy-done.3
  55.8 40.7 %shard_map.189 = (bf16[128,2048]{1,0:T(8,128)(2,1)S(1)}, bf16[8,128,256]{2,1,0:T(8,128)(2,1)S(1)}, bf16[8,128,256]{2,1,0:T(8,128)(2,1)S(1)}) custom-call(bf16[8,64,2048]{2,1,0:T(8,128)(2,1)S(1)} %bitcast.147, bf16[8,128,64]{2,1,0:T(8,128)(2,1)S(1)} %copy.53.comb, bf16[128,2048]{1,0:T(8,128)(2,1)S(1)} %copy-done.3, bf16[128,256]{1,0:T(8,128)(2,1)S(1)} %copy-done.8, ...), custom_call_target="tpu_custom_call" | custom-call | tf_op jit(solution)/shard_map/pallas_call | solution.py:283
  96.5 0.8 copy-done.4
  97.3 0.8 copy-done.5
  98.1 0.8 copy-done.6
  99.2 1.3 multiply_reduce_fusion.1
  100.5 0.9 constant_dynamic-slice_fusion
  101.4 1.7 %fusion.33 = f32[128,256]{1,0:T(8,128)S(1)} fusion(bf16[128,2048]{1,0:T(8,128)(2,1)} %copy-done.4, bf16[2048,256]{1,0:T(8,128)(2,1)} %param.20), kind=kOutput, calls=%fused_computation.90 | convolution fusion | flops 134217728 | bytes 1703936 | tf_op jit(solution)/shard_map/dot_general | solution.py:409
  103.2 0.3 convolution_convert_fusion.1.refs_1_
  103.5 16.8 %shard_map.190 = (bf16[8,4,32,256]{3,2,1,0:T(8,128)(2,1)S(1)}, bf16[8,128,256]{2,1,0:T(8,128)(2,1)S(1)}) custom-call(bf16[8,32,256]{2,1,0:T(8,128)(2,1)S(1)} %bitcast.153, bf16[128,256]{1,0:T(8,128)(2,1)S(1)} %convolution_convert_fusion.1.refs_1_), custom_call_target="tpu_custom_call" | custom-call | tf_op jit(solution)/shard_map/pallas_call | solution.py:283
  120.3 0.2 multiply_reduce_fusion
  120.7 0.2 convolution_select_fusion.1
  120.9 0.2 fusion.27
  121.1 0.3 fusion.3
  121.4 0.2 convolution_bitcast_fusion.4
  121.6 0.3 convolution_bitcast_fusion.5
  121.9 0.7 fusion.26
  122.6 0.9 convolution_add_fusion.1
  123.5 0.3 convolution_select_fusion
  123.8 0.4 fusion.34
  124.2 0.4 fusion.2
  124.6 0.7 copy.59
  125.3 1.0 convolution_bitcast_fusion.3
  126.4 3.8 %convolution_bitcast_fusion.1 = f32[1,2048,256]{2,1,0:T(8,128)} fusion(bf16[512,2048]{1,0:T(8,128)(2,1)} %bitcast.157, bf16[512,256]{1,0:T(8,128)(2,1)S(1)} %copy-done.27), kind=kOutput, calls=%fused_computation.2 | convolution fusion | flops 536870912 | bytes 4456448 | tf_op jit(solution)/shard_map/dot_general | solution.py:385
  130.2 2.1 %convolution_bitcast_fusion.2 = f32[1,2048,256]{2,1,0:T(8,128)} fusion(bf16[512,2048]{1,0:T(8,128)(2,1)S(1)} %bitcast.158, bf16[512,256]{1,0:T(8,128)(2,1)S(1)} %copy-done.25), kind=kOutput, calls=%fused_computation.3 | convolution fusion | flops 536870912 | bytes 4456448 | tf_op jit(solution)/shard_map/dot_general | solution.py:384
  132.3 0.2 copy-done.22
  132.4 2.1 %convolution_bitcast_fusion = f32[1,256,2048]{2,1,0:T(8,128)} fusion(bf16[512,2048]{1,0:T(8,128)(2,1)S(1)} %bitcast.149, f32[512,256]{1,0:T(8,128)S(1)} %copy-done.20, f32[512,256]{1,0:T(8,128)S(1)} %copy-done.22), kind=kOutput, calls=%fused_computation.1 | convolution fusion | flops 537657344 | bytes 5242880 | tf_op jit(solution)/shard_map/dot_general | solution.py:386
  (67 shorter events, 1.0 us)
Async XLA Ops:
  0.6 46.7 %copy-start = (bf16[1,2048,256]{2,1,0:T(8,128)(2,1)S(1)}, bf16[1,2048,256]{2,1,0:T(8,128)(2,1)}, u32[]{:S(2)}) copy-start(bf16[1,2048,256]{2,1,0:T(8,128)(2,1)} %param.17) | copy-start | bytes 3145732
  0.6 46.0 %copy-start.15 = (bf16[1,2048,256]{2,1,0:T(8,128)(2,1)S(1)}, bf16[1,2048,256]{2,1,0:T(8,128)(2,1)}, u32[]{:S(2)}) copy-start(bf16[1,2048,256]{2,1,0:T(8,128)(2,1)} %param.18) | copy-start | bytes 3145732
  6.4 46.0 %copy-start.11 = (f32[128,128]{1,0:T(8,128)}, f32[128,128]{1,0:T(8,128)S(1)}, u32[]{:S(2)}) copy-start(f32[128,128]{1,0:T(8,128)S(1)} %fusion.23) | copy-start | bytes 196612
  46.6 1.5 %copy-start.9 = (bf16[8,4,16,2048]{3,2,1,0:T(8,128)(2,1)}, bf16[8,4,16,2048]{3,2,1,0:T(8,128)(2,1)S(1)}, u32[]{:S(2)}) copy-start(bf16[8,4,16,2048]{3,2,1,0:T(8,128)(2,1)S(1)} %get-tuple-element.16) | copy-start | bytes 6291460
  46.6 2.0 %copy-start.1 = (bf16[8,4,16,2048]{3,2,1,0:T(8,128)(2,1)}, bf16[8,4,16,2048]{3,2,1,0:T(8,128)(2,1)S(1)}, u32[]{:S(2)}) copy-start(bf16[8,4,16,2048]{3,2,1,0:T(8,128)(2,1)S(1)} %get-tuple-element.17) | copy-start | bytes 6291460
  47.4 2.8 %copy-start.19 = (f32[512,256]{1,0:T(8,128)}, f32[512,256]{1,0:T(8,128)S(1)}, u32[]{:S(2)}) copy-start(f32[512,256]{1,0:T(8,128)S(1)} %fusion.10) | copy-start | bytes 1572868
  47.4 2.0 %copy-start.28 = (bf16[1,256,2048]{2,1,0:T(8,128)(2,1)S(1)}, bf16[1,256,2048]{2,1,0:T(8,128)(2,1)}, u32[]{:S(2)}) copy-start(bf16[1,256,2048]{2,1,0:T(8,128)(2,1)} %param.19) | copy-start | bytes 3145732
  48.1 2.1 %copy-start.21 = (f32[512,256]{1,0:T(8,128)}, f32[512,256]{1,0:T(8,128)S(1)}, u32[]{:S(2)}) copy-start(f32[512,256]{1,0:T(8,128)S(1)} %fusion.7) | copy-start | bytes 1572868
  50.2 0.8 copy-start.24
  50.2 0.8 copy-start.26
  50.2 1.4 %copy-start.16 = (bf16[1,2048,256]{2,1,0:T(8,128)(2,1)S(1)}, bf16[1,2048,256]{2,1,0:T(8,128)(2,1)}, u32[]{:S(2)}) copy-start(bf16[1,2048,256]{2,1,0:T(8,128)(2,1)} %param.18) | copy-start | bytes 3145732
  51.7 0.8 copy-start.13
  51.7 0.9 copy-start.17
  51.7 3.1 %copy-start.8 = (bf16[128,256]{1,0:T(8,128)(2,1)S(1)}, bf16[128,256]{1,0:T(8,128)(2,1)}, u32[]{:S(2)}) copy-start(bf16[128,256]{1,0:T(8,128)(2,1)} %mix.1) | copy-start | bytes 196612
  54.7 1.0 copy-start.3
  96.5 0.8 copy-start.4
  97.3 0.8 copy-start.5
  98.1 0.8 copy-start.6
  98.9 4.2 %copy-start.12 = (f32[128,128]{1,0:T(8,128)S(1)}, f32[128,128]{1,0:T(8,128)}, u32[]{:S(2)}) copy-start(f32[128,128]{1,0:T(8,128)} %copy-done.11) | copy-start | bytes 196612
  98.9 4.2 %copy-start.23 = (bf16[128,128]{1,0:T(8,128)(2,1)S(1)}, bf16[128,128]{1,0:T(8,128)(2,1)}, u32[]{:S(2)}) copy-start(bf16[128,128]{1,0:T(8,128)(2,1)} %param.22) | copy-start | bytes 98308
  99.2 21.5 %copy-start.18 = (bf16[128,256]{1,0:T(8,128)(2,1)S(1)}, bf16[128,256]{1,0:T(8,128)(2,1)}, u32[]{:S(2)}) copy-start(bf16[128,256]{1,0:T(8,128)(2,1)} %param.24) | copy-start | bytes 196612
  100.5 20.4 %copy-start.14 = (bf16[128,128]{1,0:T(8,128)(2,1)S(1)}, bf16[128,128]{1,0:T(8,128)(2,1)}, u32[]{:S(2)}) copy-start(bf16[128,128]{1,0:T(8,128)(2,1)} %param.23) | copy-start | bytes 98308
  120.3 5.0 %copy-start.7 = (bf16[8,128,256]{2,1,0:T(8,128)(2,1)S(1)}, bf16[8,128,256]{2,1,0:T(8,128)(2,1)}, u32[]{:S(2)}) copy-start(bf16[8,128,256]{2,1,0:T(8,128)(2,1)} %copy-done.6) | copy-start | bytes 1572868
  121.1 5.2 %copy-start.27 = (bf16[512,256]{1,0:T(8,128)(2,1)S(1)}, bf16[512,256]{1,0:T(8,128)(2,1)}, u32[]{:S(2)}) copy-start(bf16[512,256]{1,0:T(8,128)(2,1)} %copy-done.26) | copy-start | bytes 786436
  126.4 3.8 %copy-start.10 = (bf16[8,4,16,2048]{3,2,1,0:T(8,128)(2,1)S(1)}, bf16[8,4,16,2048]{3,2,1,0:T(8,128)(2,1)}, u32[]{:S(2)}) copy-start(bf16[8,4,16,2048]{3,2,1,0:T(8,128)(2,1)} %copy-done.9) | copy-start | bytes 6291460
  126.4 3.8 %copy-start.25 = (bf16[512,256]{1,0:T(8,128)(2,1)S(1)}, bf16[512,256]{1,0:T(8,128)(2,1)}, u32[]{:S(2)}) copy-start(bf16[512,256]{1,0:T(8,128)(2,1)} %copy-done.24) | copy-start | bytes 786436
  130.2 2.1 %copy-start.2 = (bf16[8,4,16,2048]{3,2,1,0:T(8,128)(2,1)S(1)}, bf16[8,4,16,2048]{3,2,1,0:T(8,128)(2,1)}, u32[]{:S(2)}) copy-start(bf16[8,4,16,2048]{3,2,1,0:T(8,128)(2,1)} %copy-done.1) | copy-start | bytes 6291460
  130.2 2.1 %copy-start.20 = (f32[512,256]{1,0:T(8,128)S(1)}, f32[512,256]{1,0:T(8,128)}, u32[]{:S(2)}) copy-start(f32[512,256]{1,0:T(8,128)} %copy-done.19) | copy-start | bytes 1572868
  130.2 2.2 %copy-start.22 = (f32[512,256]{1,0:T(8,128)S(1)}, f32[512,256]{1,0:T(8,128)}, u32[]{:S(2)}) copy-start(f32[512,256]{1,0:T(8,128)} %copy-done.21) | copy-start | bytes 1572868
where the time goes:
time: 136 us; the launch traced here: 135 us
  Pallas kernels  96.3 us (71%)
  matrix products  22.1 us (16%)
  local copies, waits for them, and re-layouts  9.85 us (7%)
  other arithmetic  5.07 us (4%)
    pallas_call x3, Pallas kernels, call(): pl.pallas_call(kernel, out_shape=out_shape, in_specs=in_specs, out_specs=...  96.3 us
    unnamed x60, local copies, waits for them, and re-layouts  7.42 us
    dot_general x1, matrix products, per_device(): lax.dot_general(got_x, up_cot, over, preferred_element_type=f32)[None]  3.8 us

commit v1 on v0

--- a/solution.py
+++ b/solution.py
@@ -292,7 +292,7 @@
     )(*operands)
 
 
-def per_device(
+def spread_plan(
     expert_in, out_cot, route_ids, route_weights, w_gate, w_up, w_down, w_out,
     mixed_heads, queries, keys, values, log_decay,
 ):
@@ -467,6 +467,556 @@
     )
 
 
+class Copies:
+    def __init__(self, send, recv):
+        self.send, self.recv = send, recv
+
+
+def dot(a, b, dims, exact=False):
+    return lax.dot_general(
+        a, b, (dims, ((), ())), precision=EXACT if exact else None, preferred_element_type=jnp.float32
+    )
+
+
+NN, NT, TN = ((1,), (0,)), ((1,), (1,)), ((0,), (0,))
+
+
+def whole_kernel(n_sp, n_tp, *refs):
+    bf16, f32 = jnp.bfloat16, jnp.float32
+    given, refs = refs[:13], refs[13:]
+    outs, refs = refs[:8], refs[8:]
+    x_hbm, dy_hbm, ids, weights, *_ = given
+    grad_gate, grad_up, grad_down, grad_proj, grad_q, grad_k, grad_v, grad_decay = outs
+    (
+        x_in, dy_in, wg, wu, wd, wo, mixed, qv, kv, vv, gv,
+        pos_t, wt, comb, xs, dys, gx, gdy, cots, hid, part, in1, out1, in2, out2, ret,
+        mid, gmix, gcols, dall, fsend, frecv, usend, urecv, ftot, fpre, utot, upre,
+        head, qd_s, kg_s, ke_s, sc_s, qc_s, kc_s, gv_s, cum_s,
+        load, own_sem, *sems,
+    ) = refs
+    pairs = [Copies(a, b) for a, b in zip(sems[::2], sems[1::2])]
+    (
+        c_first, c_across, c_beside, c_relay, c_sum, c_mix, c_fwd, c_half, c_cross, c_back,
+        c_share, c_rev, d_first, d_across, d_beside, d_relay,
+    ) = pairs
+    me, tp = lax.axis_index("sp"), lax.axis_index("tp")
+    far = lax.rem(tp + n_tp // 2, n_tp)
+    near = tp + 1 - 2 * lax.rem(tp, 2)
+    near_far = lax.rem(near + n_tp // 2, n_tp)
+    tok, width = x_in.shape
+    share = xs.shape[1]
+    cap = share * n_tp
+    quarter = width // n_tp
+    piece = width // n_sp
+    rows = tok // n_tp
+    bits = n_sp.bit_length() - 1
+
+    sources = (x_hbm, dy_hbm) + tuple(given[4:])
+    places = (x_in, dy_in, wg, wu, wd, wo, mixed, qv, kv, vv, gv)
+
+    def fetch(i):
+        src = sources[i].at[0] if len(sources[i].shape) == 3 else sources[i]
+        return pltpu.make_async_copy(src, places[i], load.at[i])
+
+    for i in range(len(places)):
+        fetch(i).start()
+
+    barrier = pltpu.get_barrier_semaphore()
+
+    def hello(i):
+        pl.semaphore_signal(
+            barrier, inc=1, device_id=(lax.rem(me + i, n_sp), tp), device_id_type=MESH
+        )
+
+    loop(1, n_sp, hello)
+    for other in (far, near):
+        pl.semaphore_signal(barrier, inc=1, device_id=(me, other), device_id_type=MESH)
+
+    def flip(m):
+        out = 0
+        for b in range(bits):
+            a, c = lax.rem(me // (1 << b), 2), lax.rem(m // (1 << b), 2)
+            out = out + (1 << b) * (a + c - 2 * a * c)
+        return out
+
+    def columns(block):
+        return pl.ds(pl.multiple_of(block * quarter, quarter), quarter)
+
+    lane = lax.broadcasted_iota(jnp.int32, (tok, 128), 1)
+    down = lax.broadcasted_iota(jnp.int32, (tok, tok), 0)
+    across_i = lax.broadcasted_iota(jnp.int32, (tok, tok), 1)
+    first_hit = ids[:, 0:1] == lane
+    weight = jnp.where(first_hit, weights[:, 0:1], 0.0)
+    hit = jnp.where(first_hit, 1.0, 0.0)
+    for j in range(1, ids.shape[1]):
+        hit_j = ids[:, j : j + 1] == lane
+        weight = weight + jnp.where(hit_j, weights[:, j : j + 1], 0.0)
+        hit = hit + jnp.where(hit_j, 1.0, 0.0)
+    below = jnp.where(across_i < down, 1.0, 0.0).astype(bf16)
+    rank = dot(below, hit.astype(bf16), NN)
+    pos = jnp.where(hit > 0.5, rank, -1.0)
+    pos_t[...] = jnp.transpose(pos)
+    wt[...] = jnp.transpose(weight)
+    slot_lane = lax.broadcasted_iota(jnp.int32, (tok, cap), 1).astype(f32)
+    for e in range(n_sp):
+        comb[:, e * cap : (e + 1) * cap] = jnp.where(pos[:, e : e + 1] == slot_lane, 1.0, 0.0).astype(bf16)
+
+    fetch(0).wait()
+    fetch(1).wait()
+
+    def chosen(e, start, count):
+        want = (lax.broadcasted_iota(jnp.int32, (count, tok), 0) + start).astype(f32)
+        match = pos_t[pl.ds(e, 1), :] == want
+        scale = jnp.sum(jnp.where(match, wt[pl.ds(e, 1), :], 0.0), axis=1, keepdims=True)
+        return jnp.where(match, 1.0, 0.0), scale
+
+    found = [chosen(e, tp * share, share) for e in range(n_sp)]
+    pick = jnp.concatenate([a for a, _ in found], axis=0).astype(bf16)
+    scale = jnp.concatenate([b for _, b in found], axis=0)
+    xs[...] = dot(pick, x_in[...], NN).astype(bf16).reshape(n_sp, share, width)
+    dys[...] = (scale * dot(pick, dy_in[...], NN)).astype(bf16).reshape(n_sp, share, width)
+
+    pl.semaphore_wait(barrier, n_sp + 1)
+
+    row_pairs = ((xs, gx), (dys, gdy))
+
+    def first(j, p, slot):
+        return remote(
+            row_pairs[j][0].at[p], row_pairs[j][1].at[slot, tp],
+            c_first.send.at[j, p], c_first.recv.at[j, slot], (p, tp),
+        )
+
+    def passing(copies, j, p, block, device):
+        ref = row_pairs[j][1].at[p, block]
+        return remote(ref, ref, copies.send.at[j, p], copies.recv.at[j, p], (me, device))
+
+    def across(j, p, block):
+        return passing(c_across, j, p, block, far)
+
+    def beside(j, p, block):
+        return passing(c_beside, j, p, block, near)
+
+    def relay(j, p, block):
+        return passing(c_relay, j, p, block, near)
+
+    def dispatch(m):
+        p = flip(m)
+        for j in (0, 1):
+            first(j, p, me).start()
+
+    loop(1, n_sp, dispatch)
+
+    own_pick, own_scale = chosen(me, 0, cap)
+    own_pick = own_pick.astype(bf16)
+    gx[me] = dot(own_pick, x_in[...], NN).astype(bf16).reshape(n_tp, share, width)
+    gdy[me] = (own_scale * dot(own_pick, dy_in[...], NN)).astype(bf16).reshape(n_tp, share, width)
+
+    for i in range(6, 11):
+        fetch(i).wait()
+    causal = across_i <= down
+    lower = jnp.where(causal, 1.0, 0.0)
+    cum = dot(lower, gv[...], NN, True)
+    total_decay = cum[tok - 1 : tok, :]
+    cum_s[...] = cum
+    dall[me] = jnp.broadcast_to(total_decay, dall.shape[1:])
+
+    def decay(p, slot):
+        return remote(dall.at[me], dall.at[slot], c_sum.send.at[p], c_sum.recv.at[slot], (p, tp))
+
+    def send_decay(m):
+        decay(flip(m), me).start()
+
+    loop(1, n_sp, send_decay)
+    key = kv[...].astype(f32)
+    val = vv[...].astype(f32)
+    qd_s[...] = qv[...].astype(f32) * jnp.exp(cum)
+    kg_s[...] = key * jnp.exp(-cum)
+    ke_s[...] = key * jnp.exp(total_decay - cum)
+    ftot[...] = dot(val, ke_s[...], TN, True)
+    fpre[...] = jnp.zeros_like(fpre)
+
+    def hop(copies, held, got, k):
+        partner = me + (1 << k) * (1 - 2 * lax.rem(me // (1 << k), 2))
+        return remote(held.at[k], got.at[k], copies.send.at[k], copies.recv.at[k], (partner, tp))
+
+    def give(copies, held, got, total, k):
+        held[k] = total[...].astype(bf16)
+        hop(copies, held, got, k).start()
+
+    def decay_over(low, high):
+        table = dall[:, 0, :]
+        index = lax.broadcasted_iota(jnp.int32, table.shape, 0)
+        picked = jnp.where((index >= low) & (index < high), table, 0.0)
+        return jnp.exp(jnp.sum(picked, axis=0, keepdims=True))
+
+    def span(k):
+        size = 1 << k
+        base = me - lax.rem(me, size)
+        upper = lax.rem(me // size, 2)
+        return base, base + size, upper
+
+    def forward_merge(k):
+        hop(c_fwd, fsend, frecv, k).wait_recv()
+        low, high, upper = span(k)
+        got = frecv[k].astype(f32)
+        is_upper = upper == 1
+        fpre[...] = fpre[...] + jnp.where(is_upper, decay_over(low, me), 0.0) * got
+        mine = jnp.where(is_upper, 1.0, decay_over(low + (1 << k), high + (1 << k)))
+        theirs = jnp.where(is_upper, decay_over(low, high), 1.0)
+        ftot[...] = mine * ftot[...] + theirs * got
+
+    def reverse_merge(k):
+        hop(c_rev, usend, urecv, k).wait_recv()
+        low, high, upper = span(k)
+        got = urecv[k].astype(f32)
+        is_upper = upper == 1
+        upre[...] = upre[...] + jnp.where(is_upper, 0.0, decay_over(me + 1, high)) * got
+        mine = jnp.where(is_upper, decay_over(low - (1 << k), low), 1.0)
+        theirs = jnp.where(is_upper, 1.0, decay_over(low, high))
+        utot[...] = mine * utot[...] + theirs * got
+
+    strides = [n_sp >> (k + 1) for k in range(bits)]
+
+    def mix_hop(k, base, c):
+        block = lax.rem(base, 2 * strides[k]) + c * 2 * strides[k]
+        block = lax.rem(block, n_sp)
+        partner = me + strides[k] * (1 - 2 * lax.rem(me // strides[k], 2))
+        ref = gmix.at[block]
+        return remote(ref, ref, c_mix.send.at[k, c], c_mix.recv.at[block], (partner, tp))
+
+    def widen(k):
+        def one(c):
+            mix_hop(k, me, c).start()
+
+        loop(0, n_sp // (2 * strides[k]), one)
+
+    def arrive(k):
+        partner = me + strides[k] * (1 - 2 * lax.rem(me // strides[k], 2))
+
+        def one(c):
+            mix_hop(k, partner, c).wait_recv()
+            mix_hop(k, me, c).wait_send()
+
+        loop(0, n_sp // (2 * strides[k]), one)
+
+    own_mix = pltpu.make_async_copy(mixed, gmix.at[me], own_sem)
+    own_mix.start()
+    own_mix.wait()
+    widen(0)
+    give(c_fwd, fsend, frecv, ftot, 0)
+    sc_s[...] = jnp.where(causal, dot(qd_s[...], kg_s[...], NT, True), 0.0)
+    for i in range(2, 6):
+        fetch(i).wait()
+
+    def half(j, p):
+        block = near if j == 0 else near_far
+        return remote(
+            part.at[p, :, columns(block)], in1.at[p, j], c_half.send.at[j, p], c_half.recv.at[j, p], (me, near)
+        )
+
+    def cross(p):
+        return remote(out1.at[p], in2.at[p], c_cross.send.at[p], c_cross.recv.at[p], (me, far))
+
+    def back(p, slot):
+        return remote(out2.at[p], ret.at[slot], c_back.send.at[p], c_back.recv.at[slot], (p, tp))
+
+    def expert(m):
+        p = flip(m)
+
+        @pl.when(m > 0)
+        def _():
+            for j in (0, 1):
+                beside(j, p, near).wait_recv()
+                relay(j, p, near_far).wait_recv()
+
+        x = gx[p].reshape(cap, width)
+        dy = gdy[p].reshape(cap, width)
+        gate = dot(x, wg[...], NN)
+        up = dot(x, wu[...], NN)
+        hidden_cot = dot(dy, wd[...], NT)
+        sig = jax.nn.sigmoid(gate)
+        hid[p] = (gate * sig * up).astype(bf16)
+        gate_cot = (hidden_cot * up * sig * (1.0 + gate * (1.0 - sig))).astype(bf16)
+        up_cot = (hidden_cot * gate * sig).astype(bf16)
+        units = gate_cot.shape[1]
+        cots[p, :, :units] = gate_cot
+        cots[p, :, units:] = up_cot
+        part[p] = (dot(gate_cot, wg[...], NT) + dot(up_cot, wu[...], NT)).astype(bf16)
+        for j in (1, 0):
+            half(j, p).start()
+
+    def step(i):
+        @pl.when((i >= 1) & (i < n_sp))
+        def _():
+            p = flip(i)
+            for j in (0, 1):
+                first(j, p, p).wait_recv()
+                across(j, p, tp).start()
+                beside(j, p, tp).start()
+
+        @pl.when((i >= 2) & (i < n_sp + 2))
+        def _():
+            expert(i - 2)
+
+        @pl.when((i >= 2) & (i < n_sp + 1))
+        def _():
+            p = flip(i - 1)
+            for j in (0, 1):
+                across(j, p, far).wait_recv()
+                relay(j, p, far).start()
+
+        @pl.when((i >= 3) & (i < n_sp + 3))
+        def _():
+            p = flip(i - 3)
+            half(1, p).wait_recv()
+            mine = part[p, :, columns(far)].astype(f32)
+            out1[p] = (mine + in1[p, 1].astype(f32)).astype(bf16)
+            cross(p).start()
+
+        @pl.when(i >= 4)
+        def _():
+            p = flip(i - 4)
+            half(0, p).wait_recv()
+            cross(p).wait_recv()
+            mine = part[p, :, columns(tp)].astype(f32)
+            mine = mine + in1[p, 0].astype(f32)
+            out2[p] = (mine + in2[p].astype(f32)).astype(bf16)
+
+            @pl.when(i > 4)
+            def _():
+                back(p, me).start()
+
+    loop(1, 4, step)
+
+    def wait_decay(m):
+        p = flip(m)
+        decay(p, p).wait_recv()
+
+    loop(1, n_sp, wait_decay)
+    forward_merge(0)
+    for k in range(1, bits):
+        give(c_fwd, fsend, frecv, ftot, k)
+        loop(2 + 2 * k, 4 + 2 * k, step)
+        forward_merge(k)
+    loop(2 + 2 * bits, n_sp + 4, step)
+    ret[me] = out2[me]
+    arrive(0)
+    for k in range(1, bits):
+        widen(k)
+        if k < bits - 1:
+            arrive(k)
+
+    all_x = gx.reshape(n_sp * cap, width)
+    all_dy = gdy.reshape(n_sp * cap, width)
+    tile = 256
+
+    def weight_grad(b):
+        at = pl.ds(pl.multiple_of(b * tile, tile), tile)
+        both = cots[...].reshape(n_sp * cap, cots.shape[2])
+        units = cots.shape[2] // 2
+        grads = dot(all_x[:, at], both, TN)
+        grad_gate[at, :] = grads[:, :units]
+        grad_up[at, :] = grads[:, units:]
+
+    def down_grad(b):
+        at = pl.ds(pl.multiple_of(b * tile, tile), tile)
+        grad_down[:, at] = dot(hid[...].reshape(n_sp * cap, hid.shape[2]), all_dy[:, at], TN)
+
+    loop(0, width // tile, weight_grad)
+
+    def wait_back(m):
+        p = flip(m)
+        back(p, p).wait_recv()
+
+    loop(1, n_sp, wait_back)
+    acc = dot(comb[...], ret[...].reshape(n_sp * cap, quarter), NN)
+    mid[:, columns(tp)] = (acc + dy_in[:, columns(tp)].astype(f32)).astype(bf16)
+
+    def spread(k, block, device):
+        ref = mid.at[:, columns(block)]
+        return remote(ref, ref, c_share.send.at[k], c_share.recv.at[k], (me, device))
+
+    def project(block):
+        at = pl.ds(pl.multiple_of(block * quarter, quarter), quarter)
+        return dot(mid[:, columns(block)], wo[at, :], NN)
+
+    spread(0, tp, far).start()
+    spread(1, tp, near).start()
+    head[...] = project(tp)
+    spread(1, near, near).wait_recv()
+    head[...] += project(near)
+    spread(0, far, far).wait_recv()
+    spread(2, far, near).start()
+    head[...] += project(far)
+    spread(2, near_far, near).wait_recv()
+    head[...] += project(near_far)
+
+    utot[...] = dot(head[...], qd_s[...], TN, True)
+    upre[...] = jnp.zeros_like(upre)
+    give(c_rev, usend, urecv, utot, 0)
+
+    def col_first(p, slot):
+        at = pl.ds(pl.multiple_of(p * piece, piece), piece)
+        mine = pl.ds(pl.multiple_of(tp * rows, rows), rows)
+        return remote(
+            mid.at[mine, at], gcols.at[slot, tp], d_first.send.at[p], d_first.recv.at[slot], (p, tp)
+        )
+
+    def col_pass(copies, p, block, device):
+        ref = gcols.at[p, block]
+        return remote(ref, ref, copies.send.at[p], copies.recv.at[p], (me, device))
+
+    def send_cols(m):
+        col_first(flip(m), me).start()
+
+    loop(1, n_sp, send_cols)
+    own_at = pl.ds(pl.multiple_of(me * piece, piece), piece)
+    gcols[me] = mid[:, own_at].reshape(n_tp, rows, piece)
+    scores_cot = jnp.where(causal, dot(head[...], vv[...].astype(f32), NT, True), 0.0)
+    qc_s[...] = dot(scores_cot, kg_s[...], NN, True) + dot(head[...], fpre[...], NN, True)
+    reverse_merge(0)
+    give(c_rev, usend, urecv, utot, 1)
+    kc_s[...] = dot(scores_cot, qd_s[...], TN, True)
+    gv_s[...] = dot(sc_s[...], head[...], TN, True)
+    for k in range(1, bits):
+        reverse_merge(k)
+        if k < bits - 1:
+            give(c_rev, usend, urecv, utot, k + 1)
+
+        if k == 1:
+            def col_forward(m):
+                p = flip(m)
+                col_first(p, p).wait_recv()
+                col_pass(d_across, p, tp, far).start()
+                col_pass(d_beside, p, tp, near).start()
+
+            loop(1, n_sp, col_forward)
+            loop(0, width // tile, down_grad)
+
+            def col_relay(m):
+                p = flip(m)
+                col_pass(d_across, p, far, far).wait_recv()
+                col_pass(d_relay, p, far, near).start()
+
+            loop(1, n_sp, col_relay)
+
+    carry, enter = upre[...], fpre[...]
+    cum = cum_s[...]
+    total_decay = cum[tok - 1 : tok, :]
+    val = vv[...].astype(f32)
+    ke_cot = dot(val, carry, NN, True)
+    grad_v[...] = (gv_s[...] + dot(ke_s[...], carry, NT, True)).astype(bf16)
+    end = ke_cot * ke_s[...]
+    c_cot = qc_s[...] * qd_s[...] - kc_s[...] * kg_s[...] - end
+    last = jnp.sum(end, axis=0, keepdims=True) + jnp.exp(total_decay) * jnp.sum(
+        carry * enter, axis=0, keepdims=True
+    )
+    grad_decay[...] = dot(lower, c_cot, TN, True) + last
+    grad_q[...] = (qc_s[...] * jnp.exp(cum)).astype(bf16)
+    grad_k[...] = (kc_s[...] * jnp.exp(-cum) + ke_cot * jnp.exp(total_decay - cum)).astype(bf16)
+
+    arrive(bits - 1)
+
+    def col_finish(m):
+        p = flip(m)
+        col_pass(d_beside, p, near, near).wait_recv()
+        col_pass(d_relay, p, near_far, near).wait_recv()
+
+    loop(1, n_sp, col_finish)
+    grad_proj[...] = dot(
+        gcols[...].reshape(n_sp * tok, piece), gmix[...].reshape(n_sp * tok, gmix.shape[2]), TN
+    )
+
+    def finish(m):
+        p = flip(m)
+        decay(p, me).wait_send()
+        back(p, me).wait_send()
+        col_first(p, me).wait_send()
+        col_pass(d_across, p, tp, far).wait_send()
+        col_pass(d_beside, p, tp, near).wait_send()
+        col_pass(d_relay, p, far, near).wait_send()
+        for j in (0, 1):
+            first(j, p, me).wait_send()
+            across(j, p, tp).wait_send()
+            beside(j, p, tp).wait_send()
+            relay(j, p, far).wait_send()
+
+    loop(1, n_sp, finish)
+
+    def finish_return(m):
+        p = flip(m)
+        cross(p).wait_send()
+        for j in (0, 1):
+            half(j, p).wait_send()
+
+    loop(0, n_sp, finish_return)
+    for k in range(bits):
+        hop(c_fwd, fsend, frecv, k).wait_send()
+        hop(c_rev, usend, urecv, k).wait_send()
+    spread(0, tp, far).wait_send()
+    spread(1, tp, near).wait_send()
+    spread(2, far, near).wait_send()
+
+
+def whole_plan(*args):
+    bf16, f32 = jnp.bfloat16, jnp.float32
+    n_sp, n_tp = lax.axis_size("sp"), lax.axis_size("tp")
+    expert_in, route_ids, w_gate = args[0], args[2], args[4]
+    tok, width = expert_in.shape
+    units = w_gate.shape[2]
+    cap = 2 * route_ids.shape[1] * tok // n_sp
+    share, quarter, piece = cap // n_tp, width // n_tp, width // n_sp
+    dv = args[11].shape[1]
+    bits = n_sp.bit_length() - 1
+    mem = pltpu.VMEM
+    held = [
+        mem(a.shape[1:] if a.ndim == 3 else a.shape, a.dtype) for a in args[:2] + args[4:]
+    ]
+    state = (dv, DK)
+    scratch = held + [
+        mem((128, tok), f32), mem((128, tok), f32), mem((tok, n_sp * cap), bf16),
+        mem((n_sp, share, width), bf16), mem((n_sp, share, width), bf16),
+        mem((n_sp, n_tp, share, width), bf16), mem((n_sp, n_tp, share, width), bf16),
+        mem((n_sp, cap, 2 * units), bf16), mem((n_sp, cap, units), bf16), mem((n_sp, cap, width), bf16),
+        mem((n_sp, 2, cap, quarter), bf16),
+    ] + [mem((n_sp, cap, quarter), bf16)] * 4 + [
+        mem((tok, width), bf16), mem((n_sp,) + args[8].shape, bf16), mem((n_sp, n_tp, tok // n_tp, piece), bf16),
+        mem((n_sp, 8, DK), f32),
+    ] + [mem((bits,) + state, bf16)] * 4 + [mem(state, f32)] * 4 + [mem((tok, dv), f32)] + [
+        mem((tok, DK), f32)
+    ] * 3 + [mem((tok, tok), f32), mem((tok, DK), f32), mem((tok, DK), f32), mem((tok, dv), f32), mem((tok, DK), f32)]
+    scratch += [pltpu.SemaphoreType.DMA((11,)), pltpu.SemaphoreType.DMA]
+    scratch += dma(2, n_sp) * 4 + dma(n_sp)
+    scratch += [pltpu.SemaphoreType.DMA((bits, n_sp // 2)), pltpu.SemaphoreType.DMA((n_sp,))]
+    scratch += dma(bits) + dma(2, n_sp) + dma(n_sp) * 2 + dma(3) + dma(bits) + dma(n_sp) * 4
+    shapes = [
+        ((width, units), f32), ((width, units), f32), ((units, width), f32), ((piece, args[8].shape[1]), f32),
+        (args[9].shape, bf16), (args[10].shape, bf16), (args[11].shape, bf16), (args[12].shape, f32),
+    ]
+    outs = pl.pallas_call(
+        functools.partial(whole_kernel, n_sp, n_tp),
+        out_shape=tuple(jax.ShapeDtypeStruct(s, t) for s, t in shapes),
+        in_specs=[ANY, ANY, VM, VM] + [ANY] * 9,
+        out_specs=(VM,) * 8,
+        scratch_shapes=scratch,
+        compiler_params=pltpu.CompilerParams(
+            collective_id=3, has_side_effects=True, vmem_limit_bytes=56 * 1024 * 1024
+        ),
+    )(*args)
+    return tuple(a[None] for a in outs[:3]) + tuple(outs[3:])
+
+
+def per_device(*args):
+    n_sp, n_tp = lax.axis_size("sp"), lax.axis_size("tp")
+    tok, top = args[0].shape[0], args[2].shape[1]
+    heads = args[9].shape[1] // DK
+    share = 2 * top * tok // (n_sp * n_tp)
+    aligned = share % 16 == 0 and tok // n_tp % 16 == 0 and tok == 128
+    if aligned and heads == 1 and args[4].shape[0] == 1 and n_tp == 4 and n_sp & (n_sp - 1) == 0:
+        return whole_plan(*args)
+    return spread_plan(*args)
+
+
 def solution(mesh):
     tokens, both = P("sp", None), P("sp", "tp")
     up, down = P("sp", None, "tp"), P("sp", "tp", None)

time: 136 us -> 108 us (0.79)
  matrix products: 22.1 us -> 0 us
  other arithmetic: 5.07 us -> 0 us
  local copies, waits for them, and re-layouts: 9.85 us -> 12.9 us
  Pallas kernels: 96.3 us -> 93.8 us
    dot_general x25 -> x0, matrix products: 22.1 us -> none  [the longest x1 3.8 us: per_device(): lax.dot_general(got_x, up_cot, over, preferred_element_type=f32)[None]]
    unnamed x60 -> x24, local copies, waits for them, and re-layouts: 7.42 us -> 12.9 us
    reduce_sum x6 -> x0, other arithmetic: 3.2 us -> none  [the longest x2 1.49 us: entering(): jnp.sum(scale[..., None] * pieces.astype(f32), axis=0)]
    pallas_call x3 -> x1, Pallas kernels: 96.3 us -> 93.8 us  [whole_plan(): pl.pallas_call(functools.partial(whole_kernel, n_sp, n_tp), out_shape=tup...]
where the time goes in v1:
time: 108 us; the launch traced here: 107 us
  Pallas kernels  93.8 us (87%)
  local copies, waits for them, and re-layouts  12.9 us (12%)
    pallas_call x1, Pallas kernels, whole_plan(): pl.pallas_call(functools.partial(whole_kernel, n_sp, n_tp), out_shape=tup...  93.8 us
    unnamed x24, local copies, waits for them, and re-layouts  12.9 us

profile of v1, /device:TPU:0, one launch (start us, length us, event | category | flops | bytes accessed | tf_op | source)
XLA Modules:
  0.0 107.4 jit_solution(96646092722043521)
XLA Ops:
  0.6 1.4 %copy.21.refs_2_ = s32[128,2]{1,0:T(8,128)} copy(s32[128,2]{0,1:T(2,128)} %param.15) | data formatting | bytes 2048 | tf_op args[2]
  2.0 1.4 %copy.22.refs_3_ = f32[128,2]{1,0:T(8,128)} copy(f32[128,2]{0,1:T(2,128)} %param.16) | data formatting | bytes 2048 | tf_op args[3]
  3.5 93.8 %shard_map.188 = (f32[2048,256]{1,0:T(8,128)}, f32[2048,256]{1,0:T(8,128)}, f32[256,2048]{1,0:T(8,128)}, f32[256,256]{1,0:T(8,128)}, bf16[128,128]{1,0:T(8,128)(...) custom-call(bf16[128,2048]{1,0:T(8,128)(2,1)} %refs_0_.1, ...), custom_call_target="tpu_custom_call" | custom-call | tf_op jit(solution)/shard_map/pallas_call | solution.py:996
  97.3 0.0 copy-start.1
  97.3 3.2 %copy.31 = f32[1,2048,256]{2,1,0:T(8,128)} copy(f32[1,2048,256]{2,1,0:T(8,128)} %bitcast.5) | data formatting | bytes 4194304
  100.5 0.0 copy-done.1
  100.5 0.0 copy-start
  100.5 1.3 %copy.32 = f32[1,2048,256]{2,1,0:T(8,128)} copy(f32[1,2048,256]{2,1,0:T(8,128)S(1)} %bitcast.4) | data formatting | bytes 4194304
  101.8 1.0 copy-done
  102.8 0.0 copy-start.2
  102.8 0.0 copy-start.6
  102.8 0.0 copy-start.5
  102.8 0.0 copy-start.4
  102.8 0.0 copy-start.3
  102.9 1.3 %copy.33 = f32[1,256,2048]{2,1,0:T(8,128)} copy(f32[1,256,2048]{2,1,0:T(8,128)S(1)} %bitcast.3) | data formatting | bytes 4194304
  104.2 0.0 copy-done.2
  104.2 0.7 copy.34
  104.9 0.0 copy-done.6
  104.9 0.6 copy.35
  105.5 0.0 copy-done.5
  105.5 0.6 copy.36
  106.1 0.0 copy-done.4
  106.1 0.6 copy.37
  106.8 0.0 copy-done.3
  106.8 0.6 copy.38
Async XLA Ops:
  97.3 3.2 %copy-start.1 = (f32[2048,256]{1,0:T(8,128)S(1)}, f32[2048,256]{1,0:T(8,128)}, u32[]{:S(2)}) copy-start(f32[2048,256]{1,0:T(8,128)} %get-tuple-element.17) | copy-start | bytes 6291460
  100.5 2.3 %copy-start = (f32[256,2048]{1,0:T(8,128)S(1)}, f32[256,2048]{1,0:T(8,128)}, u32[]{:S(2)}) copy-start(f32[256,2048]{1,0:T(8,128)} %get-tuple-element.18) | copy-start | bytes 6291460
  102.8 1.3 %copy-start.2 = (f32[256,256]{1,0:T(8,128)S(1)}, f32[256,256]{1,0:T(8,128)}, u32[]{:S(2)}) copy-start(f32[256,256]{1,0:T(8,128)} %get-tuple-element.35) | copy-start | bytes 786436
  102.8 2.0 %copy-start.6 = (bf16[128,128]{1,0:T(8,128)(2,1)S(1)}, bf16[128,128]{1,0:T(8,128)(2,1)}, u32[]{:S(2)}) copy-start(bf16[128,128]{1,0:T(8,128)(2,1)} %get-tuple-element.36) | copy-start | bytes 98308
  102.8 2.7 %copy-start.5 = (bf16[128,128]{1,0:T(8,128)(2,1)S(1)}, bf16[128,128]{1,0:T(8,128)(2,1)}, u32[]{:S(2)}) copy-start(bf16[128,128]{1,0:T(8,128)(2,1)} %get-tuple-element.37) | copy-start | bytes 98308
  102.8 3.3 %copy-start.4 = (bf16[128,256]{1,0:T(8,128)(2,1)S(1)}, bf16[128,256]{1,0:T(8,128)(2,1)}, u32[]{:S(2)}) copy-start(bf16[128,256]{1,0:T(8,128)(2,1)} %get-tuple-element.38) | copy-start | bytes 196612
  102.8 3.9 %copy-start.3 = (f32[128,128]{1,0:T(8,128)S(1)}, f32[128,128]{1,0:T(8,128)}, u32[]{:S(2)}) copy-start(f32[128,128]{1,0:T(8,128)} %get-tuple-element.39) | copy-start | bytes 196612

commit v2 on v1

--- a/solution.py
+++ b/solution.py
@@ -497,19 +497,20 @@
     pairs = [Copies(a, b) for a, b in zip(sems[::2], sems[1::2])]
     (
         c_first, c_across, c_beside, c_relay, c_sum, c_mix, c_fwd, c_half, c_cross, c_back,
-        c_share, c_rev, d_first, d_across, d_beside, d_relay,
+        c_share, c_rev, c_second, d_first, d_across, d_beside, d_relay,
     ) = pairs
     me, tp = lax.axis_index("sp"), lax.axis_index("tp")
     far = lax.rem(tp + n_tp // 2, n_tp)
     near = tp + 1 - 2 * lax.rem(tp, 2)
     near_far = lax.rem(near + n_tp // 2, n_tp)
     tok, width = x_in.shape
-    share = xs.shape[1]
+    share = xs.shape[2]
     cap = share * n_tp
     quarter = width // n_tp
     piece = width // n_sp
     rows = tok // n_tp
     bits = n_sp.bit_length() - 1
+    close = 2
 
     sources = (x_hbm, dy_hbm) + tuple(given[4:])
     places = (x_in, dy_in, wg, wu, wd, wo, mixed, qv, kv, vv, gv)
@@ -539,24 +540,30 @@
             out = out + (1 << b) * (a + c - 2 * a * c)
         return out
 
+    def turn(i):
+        zero = 1 - (i + n_sp - 1) // n_sp
+        is_near = lax.rem(i, 2) * (1 - i // (n_sp - 1)) + zero
+        half_way = (i + 1) // 2
+        return half_way + (1 - is_near) * (n_sp // 2 - 1)
+
+    def peer(i):
+        return flip(turn(i))
+
     def columns(block):
         return pl.ds(pl.multiple_of(block * quarter, quarter), quarter)
 
-    lane = lax.broadcasted_iota(jnp.int32, (tok, 128), 1)
     down = lax.broadcasted_iota(jnp.int32, (tok, tok), 0)
     across_i = lax.broadcasted_iota(jnp.int32, (tok, tok), 1)
-    first_hit = ids[:, 0:1] == lane
-    weight = jnp.where(first_hit, weights[:, 0:1], 0.0)
-    hit = jnp.where(first_hit, 1.0, 0.0)
-    for j in range(1, ids.shape[1]):
-        hit_j = ids[:, j : j + 1] == lane
-        weight = weight + jnp.where(hit_j, weights[:, j : j + 1], 0.0)
+    weight, hit = jnp.zeros((tok, tok), f32), jnp.zeros((tok, tok), f32)
+    for j in range(ids.shape[0]):
+        hit_j = ids[j : j + 1, :] == down
+        weight = weight + jnp.where(hit_j, weights[j : j + 1, :], 0.0)
         hit = hit + jnp.where(hit_j, 1.0, 0.0)
-    below = jnp.where(across_i < down, 1.0, 0.0).astype(bf16)
-    rank = dot(below, hit.astype(bf16), NN)
-    pos = jnp.where(hit > 0.5, rank, -1.0)
-    pos_t[...] = jnp.transpose(pos)
-    wt[...] = jnp.transpose(weight)
+    above = jnp.where(down < across_i, 1.0, 0.0).astype(bf16)
+    pos = jnp.where(hit > 0.5, dot(hit.astype(bf16), above, NN), -1.0)
+    pos_t[...] = pos
+    wt[...] = weight
+    pos = jnp.transpose(pos)
     slot_lane = lax.broadcasted_iota(jnp.int32, (tok, cap), 1).astype(f32)
     for e in range(n_sp):
         comb[:, e * cap : (e + 1) * cap] = jnp.where(pos[:, e : e + 1] == slot_lane, 1.0, 0.0).astype(bf16)
@@ -570,11 +577,11 @@
         scale = jnp.sum(jnp.where(match, wt[pl.ds(e, 1), :], 0.0), axis=1, keepdims=True)
         return jnp.where(match, 1.0, 0.0), scale
 
-    found = [chosen(e, tp * share, share) for e in range(n_sp)]
+    found = [chosen(e, block * share, share) for e in range(n_sp) for block in (tp, far)]
     pick = jnp.concatenate([a for a, _ in found], axis=0).astype(bf16)
     scale = jnp.concatenate([b for _, b in found], axis=0)
-    xs[...] = dot(pick, x_in[...], NN).astype(bf16).reshape(n_sp, share, width)
-    dys[...] = (scale * dot(pick, dy_in[...], NN)).astype(bf16).reshape(n_sp, share, width)
+    xs[...] = dot(pick, x_in[...], NN).astype(bf16).reshape(n_sp, 2, share, width)
+    dys[...] = (scale * dot(pick, dy_in[...], NN)).astype(bf16).reshape(n_sp, 2, share, width)
 
     pl.semaphore_wait(barrier, n_sp + 1)
 
@@ -582,8 +589,14 @@
 
     def first(j, p, slot):
         return remote(
-            row_pairs[j][0].at[p], row_pairs[j][1].at[slot, tp],
+            row_pairs[j][0].at[p, 0], row_pairs[j][1].at[slot, tp],
             c_first.send.at[j, p], c_first.recv.at[j, slot], (p, tp),
+        )
+
+    def second(j, p, slot):
+        return remote(
+            row_pairs[j][0].at[p, 1], row_pairs[j][1].at[slot, far],
+            c_second.send.at[j, p], c_second.recv.at[j, slot], (p, tp),
         )
 
     def passing(copies, j, p, block, device):
@@ -600,9 +613,13 @@
         return passing(c_relay, j, p, block, near)
 
     def dispatch(m):
-        p = flip(m)
+        p = peer(m)
         for j in (0, 1):
             first(j, p, me).start()
+
+            @pl.when(m < close)
+            def _():
+                second(j, p, me).start()
 
     loop(1, n_sp, dispatch)
 
@@ -721,7 +738,7 @@
         return remote(out2.at[p], ret.at[slot], c_back.send.at[p], c_back.recv.at[slot], (p, tp))
 
     def expert(m):
-        p = flip(m)
+        p = peer(m)
 
         @pl.when(m > 0)
         def _():
@@ -746,36 +763,48 @@
             half(j, p).start()
 
     def step(i):
-        @pl.when((i >= 1) & (i < n_sp))
-        def _():
-            p = flip(i)
-            for j in (0, 1):
-                first(j, p, p).wait_recv()
-                across(j, p, tp).start()
-                beside(j, p, tp).start()
-
-        @pl.when((i >= 2) & (i < n_sp + 2))
-        def _():
-            expert(i - 2)
-
-        @pl.when((i >= 2) & (i < n_sp + 1))
-        def _():
-            p = flip(i - 1)
-            for j in (0, 1):
-                across(j, p, far).wait_recv()
-                relay(j, p, far).start()
-
         @pl.when((i >= 3) & (i < n_sp + 3))
         def _():
-            p = flip(i - 3)
+            p = peer(i - 3)
             half(1, p).wait_recv()
             mine = part[p, :, columns(far)].astype(f32)
             out1[p] = (mine + in1[p, 1].astype(f32)).astype(bf16)
             cross(p).start()
 
+        @pl.when(i < n_sp)
+        def _():
+            p = peer(i)
+            for j in (0, 1):
+                first(j, p, p).wait_recv()
+
+                @pl.when(i >= close)
+                def _():
+                    across(j, p, tp).start()
+
+                beside(j, p, tp).start()
+
+        @pl.when((i >= 3) & (i < n_sp + 2))
+        def _():
+            expert(i - 2)
+
+        @pl.when((i >= 2) & (i < n_sp + 1))
+        def _():
+            p = peer(i - 1)
+            for j in (0, 1):
+
+                @pl.when(i - 1 >= close)
+                def _():
+                    across(j, p, far).wait_recv()
+
+                @pl.when(i - 1 < close)
+                def _():
+                    second(j, p, p).wait_recv()
+
+                relay(j, p, far).start()
+
         @pl.when(i >= 4)
         def _():
-            p = flip(i - 4)
+            p = peer(i - 4)
             half(0, p).wait_recv()
             cross(p).wait_recv()
             mine = part[p, :, columns(tp)].astype(f32)
@@ -786,25 +815,13 @@
             def _():
                 back(p, me).start()
 
-    loop(1, 4, step)
+    expert(0)
+    loop(1, n_sp + 4, step)
+    ret[me] = out2[me]
 
     def wait_decay(m):
         p = flip(m)
         decay(p, p).wait_recv()
-
-    loop(1, n_sp, wait_decay)
-    forward_merge(0)
-    for k in range(1, bits):
-        give(c_fwd, fsend, frecv, ftot, k)
-        loop(2 + 2 * k, 4 + 2 * k, step)
-        forward_merge(k)
-    loop(2 + 2 * bits, n_sp + 4, step)
-    ret[me] = out2[me]
-    arrive(0)
-    for k in range(1, bits):
-        widen(k)
-        if k < bits - 1:
-            arrive(k)
 
     all_x = gx.reshape(n_sp * cap, width)
     all_dy = gdy.reshape(n_sp * cap, width)
@@ -842,6 +859,11 @@
 
     spread(0, tp, far).start()
     spread(1, tp, near).start()
+    loop(1, n_sp, wait_decay)
+    forward_merge(0)
+    give(c_fwd, fsend, frecv, ftot, 1)
+    arrive(0)
+    widen(1)
     head[...] = project(tp)
     spread(1, near, near).wait_recv()
     head[...] += project(near)
@@ -870,12 +892,19 @@
         col_first(flip(m), me).start()
 
     loop(1, n_sp, send_cols)
+    for k in range(1, bits - 1):
+        arrive(k)
+        widen(k + 1)
     own_at = pl.ds(pl.multiple_of(me * piece, piece), piece)
     gcols[me] = mid[:, own_at].reshape(n_tp, rows, piece)
     scores_cot = jnp.where(causal, dot(head[...], vv[...].astype(f32), NT, True), 0.0)
-    qc_s[...] = dot(scores_cot, kg_s[...], NN, True) + dot(head[...], fpre[...], NN, True)
+    for k in range(1, bits - 1):
+        forward_merge(k)
+        give(c_fwd, fsend, frecv, ftot, k + 1)
+    qc_s[...] = dot(scores_cot, kg_s[...], NN, True)
     reverse_merge(0)
     give(c_rev, usend, urecv, utot, 1)
+    loop(0, width // tile, down_grad)
     kc_s[...] = dot(scores_cot, qd_s[...], TN, True)
     gv_s[...] = dot(sc_s[...], head[...], TN, True)
     for k in range(1, bits):
@@ -891,8 +920,6 @@
                 col_pass(d_beside, p, tp, near).start()
 
             loop(1, n_sp, col_forward)
-            loop(0, width // tile, down_grad)
-
             def col_relay(m):
                 p = flip(m)
                 col_pass(d_across, p, far, far).wait_recv()
@@ -900,7 +927,9 @@
 
             loop(1, n_sp, col_relay)
 
+    forward_merge(bits - 1)
     carry, enter = upre[...], fpre[...]
+    qc_s[...] += dot(head[...], enter, NN, True)
     cum = cum_s[...]
     total_decay = cum[tok - 1 : tok, :]
     val = vv[...].astype(f32)
@@ -928,7 +957,7 @@
     )
 
     def finish(m):
-        p = flip(m)
+        p = peer(m)
         decay(p, me).wait_send()
         back(p, me).wait_send()
         col_first(p, me).wait_send()
@@ -937,7 +966,15 @@
         col_pass(d_relay, p, far, near).wait_send()
         for j in (0, 1):
             first(j, p, me).wait_send()
-            across(j, p, tp).wait_send()
+
+            @pl.when(m >= close)
+            def _():
+                across(j, p, tp).wait_send()
+
+            @pl.when(m < close)
+            def _():
+                second(j, p, me).wait_send()
+
             beside(j, p, tp).wait_send()
             relay(j, p, far).wait_send()
 
@@ -956,6 +993,29 @@
     spread(0, tp, far).wait_send()
     spread(1, tp, near).wait_send()
     spread(2, far, near).wait_send()
+
+
+def flush_kernel(*refs):
+    count = (len(refs) - 1) // 2
+    copies = [
+        pltpu.make_async_copy(refs[i], refs[count + i], refs[-1].at[i]) for i in range(count)
+    ]
+    for copy in copies:
+        copy.start()
+    for copy in copies:
+        copy.wait()
+
+
+def flush(arrays):
+    count = len(arrays)
+    return pl.pallas_call(
+        flush_kernel,
+        out_shape=tuple(jax.ShapeDtypeStruct(a.shape, a.dtype) for a in arrays),
+        in_specs=[VM] * count,
+        out_specs=(ANY,) * count,
+        scratch_shapes=[pltpu.SemaphoreType.DMA((count,))],
+        compiler_params=pltpu.CompilerParams(vmem_limit_bytes=1024 * 1024),
+    )(*[pltpu.with_memory_space_constraint(a, pltpu.VMEM) for a in arrays])
 
 
 def whole_plan(*args):
@@ -974,8 +1034,8 @@
     ]
     state = (dv, DK)
     scratch = held + [
-        mem((128, tok), f32), mem((128, tok), f32), mem((tok, n_sp * cap), bf16),
-        mem((n_sp, share, width), bf16), mem((n_sp, share, width), bf16),
+        mem((tok, tok), f32), mem((tok, tok), f32), mem((tok, n_sp * cap), bf16),
+        mem((n_sp, 2, share, width), bf16), mem((n_sp, 2, share, width), bf16),
         mem((n_sp, n_tp, share, width), bf16), mem((n_sp, n_tp, share, width), bf16),
         mem((n_sp, cap, 2 * units), bf16), mem((n_sp, cap, units), bf16), mem((n_sp, cap, width), bf16),
         mem((n_sp, 2, cap, quarter), bf16),
@@ -988,21 +1048,22 @@
     scratch += [pltpu.SemaphoreType.DMA((11,)), pltpu.SemaphoreType.DMA]
     scratch += dma(2, n_sp) * 4 + dma(n_sp)
     scratch += [pltpu.SemaphoreType.DMA((bits, n_sp // 2)), pltpu.SemaphoreType.DMA((n_sp,))]
-    scratch += dma(bits) + dma(2, n_sp) + dma(n_sp) * 2 + dma(3) + dma(bits) + dma(n_sp) * 4
+    scratch += dma(bits) + dma(2, n_sp) + dma(n_sp) * 2 + dma(3) + dma(bits) + dma(2, n_sp) + dma(n_sp) * 4
     shapes = [
         ((width, units), f32), ((width, units), f32), ((units, width), f32), ((piece, args[8].shape[1]), f32),
         (args[9].shape, bf16), (args[10].shape, bf16), (args[11].shape, bf16), (args[12].shape, f32),
     ]
     outs = pl.pallas_call(
         functools.partial(whole_kernel, n_sp, n_tp),
-        out_shape=tuple(jax.ShapeDtypeStruct(s, t) for s, t in shapes),
+        out_shape=tuple(pltpu.VMEM(s, t) for s, t in shapes),
         in_specs=[ANY, ANY, VM, VM] + [ANY] * 9,
         out_specs=(VM,) * 8,
         scratch_shapes=scratch,
         compiler_params=pltpu.CompilerParams(
             collective_id=3, has_side_effects=True, vmem_limit_bytes=56 * 1024 * 1024
         ),
-    )(*args)
+    )(*args[:2], args[2].T, args[3].T, *args[4:])
+    outs = flush(outs)
     return tuple(a[None] for a in outs[:3]) + tuple(outs[3:])
 
 

time: 108 us -> 80 us (0.74)
  Pallas kernels: 93.8 us -> 79.2 us
  local copies, waits for them, and re-layouts: 12.9 us -> 0 us
    pallas_call x1, Pallas kernels: 93.8 us -> 76.4 us  [whole_plan(): pl.pallas_call(functools.partial(whole_kernel, n_sp, n_tp), out_shape=tup...]
    unnamed x24 -> x0, local copies, waits for them, and re-layouts: 12.9 us -> none
    pallas_call x0 -> x1, Pallas kernels: none -> 2.83 us  [flush(): pl.pallas_call(flush_kernel, out_shape=tuple((jax.ShapeDtypeStruct(a.shap...]
where the time goes in v2:
time: 80 us; the launch traced here: 79.9 us
  Pallas kernels  79.2 us (99%)
    pallas_call x1, Pallas kernels, whole_plan(): pl.pallas_call(functools.partial(whole_kernel, n_sp, n_tp), out_shape=tup...  76.4 us
    pallas_call x1, Pallas kernels, flush(): pl.pallas_call(flush_kernel, out_shape=tuple((jax.ShapeDtypeStruct(a.shap...  2.83 us

profile of v2, /device:TPU:0, one launch (start us, length us, event | category | flops | bytes accessed | tf_op | source)
XLA Modules:
  0.0 79.9 jit_solution(8092390542115758457)
XLA Ops:
  0.6 76.4 %shard_map.188 = (f32[2048,256]{1,0:T(8,128)S(1)}, f32[2048,256]{1,0:T(8,128)S(1)}, f32[256,2048]{1,0:T(8,128)S(1)}, f32[256,256]{1,0:T(8,128)S(1)}, bf16[128,12...) custom-call(bf16[128,2048]{1,0:T(8,128)(2,1)} %refs_0_.1, ...), custom_call_target="tpu_custom_call" | custom-call | tf_op jit(solution)/shard_map/pallas_call | solution.py:1056
  77.0 2.8 %shard_map.189 = (f32[2048,256]{1,0:T(8,128)}, f32[2048,256]{1,0:T(8,128)}, f32[256,2048]{1,0:T(8,128)}, f32[256,256]{1,0:T(8,128)}, bf16[128,128]{1,0:T(8,128)(...) custom-call(f32[2048,256]{1,0:T(8,128)S(1)} %get-tuple-element.24.refs_0_, ...), custom_call_target="tpu_custom_call" | custom-call | tf_op jit(solution)/shard_map/pallas_call | solution.py:1011

commit v3 on v2

--- a/solution.py
+++ b/solution.py
@@ -486,31 +486,30 @@
     given, refs = refs[:13], refs[13:]
     outs, refs = refs[:8], refs[8:]
     x_hbm, dy_hbm, ids, weights, *_ = given
-    grad_gate, grad_up, grad_down, grad_proj, grad_q, grad_k, grad_v, grad_decay = outs
+    out_gate, out_up, out_down, grad_proj, grad_q, grad_k, grad_v, grad_decay = outs
     (
         x_in, dy_in, wg, wu, wd, wo, mixed, qv, kv, vv, gv,
         pos_t, wt, comb, xs, dys, gx, gdy, cots, hid, part, in1, out1, in2, out2, ret,
         mid, gmix, gcols, dall, fsend, frecv, usend, urecv, ftot, fpre, utot, upre,
         head, qd_s, kg_s, ke_s, sc_s, qc_s, kc_s, gv_s, cum_s,
-        load, own_sem, *sems,
+        grad_gate, grad_up, grad_down, load, own_sem, put_sem, *sems,
     ) = refs
     pairs = [Copies(a, b) for a, b in zip(sems[::2], sems[1::2])]
     (
         c_first, c_across, c_beside, c_relay, c_sum, c_mix, c_fwd, c_half, c_cross, c_back,
-        c_share, c_rev, c_second, d_first, d_across, d_beside, d_relay,
+        c_share, c_rev, d_first, d_across, d_beside, d_relay,
     ) = pairs
     me, tp = lax.axis_index("sp"), lax.axis_index("tp")
     far = lax.rem(tp + n_tp // 2, n_tp)
     near = tp + 1 - 2 * lax.rem(tp, 2)
     near_far = lax.rem(near + n_tp // 2, n_tp)
     tok, width = x_in.shape
-    share = xs.shape[2]
+    share = xs.shape[1]
     cap = share * n_tp
     quarter = width // n_tp
     piece = width // n_sp
     rows = tok // n_tp
     bits = n_sp.bit_length() - 1
-    close = 2
 
     sources = (x_hbm, dy_hbm) + tuple(given[4:])
     places = (x_in, dy_in, wg, wu, wd, wo, mixed, qv, kv, vv, gv)
@@ -548,6 +547,15 @@
 
     def peer(i):
         return flip(turn(i))
+
+    others = pl.ds(0, n_sp - 1)
+
+    def whole(copies, ref):
+        recv = copies.recv.at[(0,) * len(copies.recv.shape)] if copies.recv.shape else copies.recv
+        return remote(ref, ref, copies.send, recv, (me, far))
+
+    def got_all(copies, ref):
+        whole(copies, ref).wait_recv()
 
     def columns(block):
         return pl.ds(pl.multiple_of(block * quarter, quarter), quarter)
@@ -577,11 +585,11 @@
         scale = jnp.sum(jnp.where(match, wt[pl.ds(e, 1), :], 0.0), axis=1, keepdims=True)
         return jnp.where(match, 1.0, 0.0), scale
 
-    found = [chosen(e, block * share, share) for e in range(n_sp) for block in (tp, far)]
+    found = [chosen(e, tp * share, share) for e in range(n_sp)]
     pick = jnp.concatenate([a for a, _ in found], axis=0).astype(bf16)
     scale = jnp.concatenate([b for _, b in found], axis=0)
-    xs[...] = dot(pick, x_in[...], NN).astype(bf16).reshape(n_sp, 2, share, width)
-    dys[...] = (scale * dot(pick, dy_in[...], NN)).astype(bf16).reshape(n_sp, 2, share, width)
+    xs[...] = dot(pick, x_in[...], NN).astype(bf16).reshape(n_sp, share, width)
+    dys[...] = (scale * dot(pick, dy_in[...], NN)).astype(bf16).reshape(n_sp, share, width)
 
     pl.semaphore_wait(barrier, n_sp + 1)
 
@@ -589,19 +597,17 @@
 
     def first(j, p, slot):
         return remote(
-            row_pairs[j][0].at[p, 0], row_pairs[j][1].at[slot, tp],
-            c_first.send.at[j, p], c_first.recv.at[j, slot], (p, tp),
-        )
-
-    def second(j, p, slot):
-        return remote(
-            row_pairs[j][0].at[p, 1], row_pairs[j][1].at[slot, far],
-            c_second.send.at[j, p], c_second.recv.at[j, slot], (p, tp),
+            row_pairs[j][0].at[p], row_pairs[j][1].at[slot, tp],
+            c_first.send, c_first.recv.at[j, slot], (p, tp),
         )
 
     def passing(copies, j, p, block, device):
         ref = row_pairs[j][1].at[p, block]
-        return remote(ref, ref, copies.send.at[j, p], copies.recv.at[j, p], (me, device))
+        return remote(ref, ref, copies.send, copies.recv.at[p], (me, device))
+
+    def arrived(copies, p):
+        ref = gx.at[p, pl.ds(0, 2)]
+        remote(ref, ref, copies.send, copies.recv.at[p], (me, far)).wait_recv()
 
     def across(j, p, block):
         return passing(c_across, j, p, block, far)
@@ -616,10 +622,6 @@
         p = peer(m)
         for j in (0, 1):
             first(j, p, me).start()
-
-            @pl.when(m < close)
-            def _():
-                second(j, p, me).start()
 
     loop(1, n_sp, dispatch)
 
@@ -638,7 +640,7 @@
     dall[me] = jnp.broadcast_to(total_decay, dall.shape[1:])
 
     def decay(p, slot):
-        return remote(dall.at[me], dall.at[slot], c_sum.send.at[p], c_sum.recv.at[slot], (p, tp))
+        return remote(dall.at[me], dall.at[slot], c_sum.send, c_sum.recv, (p, tp))
 
     def send_decay(m):
         decay(flip(m), me).start()
@@ -652,13 +654,18 @@
     ftot[...] = dot(val, ke_s[...], TN, True)
     fpre[...] = jnp.zeros_like(fpre)
 
-    def hop(copies, held, got, k):
+    piece_rows = ftot.shape[0] // 2
+
+    def hop(copies, held, got, k, c):
         partner = me + (1 << k) * (1 - 2 * lax.rem(me // (1 << k), 2))
-        return remote(held.at[k], got.at[k], copies.send.at[k], copies.recv.at[k], (partner, tp))
-
-    def give(copies, held, got, total, k):
-        held[k] = total[...].astype(bf16)
-        hop(copies, held, got, k).start()
+        return remote(held.at[k, c], got.at[k, c], copies.send, copies.recv.at[k, c], (partner, tp))
+
+    def lines(c):
+        return slice(c * piece_rows, (c + 1) * piece_rows)
+
+    def give(copies, held, got, total, k, c):
+        held[k, c] = total[lines(c), :].astype(bf16)
+        hop(copies, held, got, k, c).start()
 
     def decay_over(low, high):
         table = dall[:, 0, :]
@@ -672,25 +679,30 @@
         upper = lax.rem(me // size, 2)
         return base, base + size, upper
 
-    def forward_merge(k):
-        hop(c_fwd, fsend, frecv, k).wait_recv()
+    def forward_merge(k, c):
+        hop(c_fwd, fsend, frecv, k, c).wait_recv()
         low, high, upper = span(k)
-        got = frecv[k].astype(f32)
+        got = frecv[k, c].astype(f32)
         is_upper = upper == 1
-        fpre[...] = fpre[...] + jnp.where(is_upper, decay_over(low, me), 0.0) * got
+        at = lines(c)
+        fpre[at, :] = fpre[at, :] + jnp.where(is_upper, decay_over(low, me), 0.0) * got
         mine = jnp.where(is_upper, 1.0, decay_over(low + (1 << k), high + (1 << k)))
         theirs = jnp.where(is_upper, decay_over(low, high), 1.0)
-        ftot[...] = mine * ftot[...] + theirs * got
-
-    def reverse_merge(k):
-        hop(c_rev, usend, urecv, k).wait_recv()
+        ftot[at, :] = mine * ftot[at, :] + theirs * got
+
+    def reverse_merge(k, c):
         low, high, upper = span(k)
-        got = urecv[k].astype(f32)
         is_upper = upper == 1
-        upre[...] = upre[...] + jnp.where(is_upper, 0.0, decay_over(me + 1, high)) * got
+        after = jnp.where(is_upper, 0.0, decay_over(me + 1, high))
         mine = jnp.where(is_upper, decay_over(low - (1 << k), low), 1.0)
         theirs = jnp.where(is_upper, 1.0, decay_over(low, high))
-        utot[...] = mine * utot[...] + theirs * got
+        hop(c_rev, usend, urecv, k, c).wait_recv()
+        got = urecv[k, c].astype(f32)
+        at = lines(c)
+        if k < bits - 1:
+            utot[at, :] = mine * utot[at, :] + theirs * got
+            give(c_rev, usend, urecv, utot, k + 1, c)
+        upre[at, :] = upre[at, :] + after * got
 
     strides = [n_sp >> (k + 1) for k in range(bits)]
 
@@ -699,7 +711,7 @@
         block = lax.rem(block, n_sp)
         partner = me + strides[k] * (1 - 2 * lax.rem(me // strides[k], 2))
         ref = gmix.at[block]
-        return remote(ref, ref, c_mix.send.at[k, c], c_mix.recv.at[block], (partner, tp))
+        return remote(ref, ref, c_mix.send, c_mix.recv.at[block], (partner, tp))
 
     def widen(k):
         def one(c):
@@ -712,7 +724,6 @@
 
         def one(c):
             mix_hop(k, partner, c).wait_recv()
-            mix_hop(k, me, c).wait_send()
 
         loop(0, n_sp // (2 * strides[k]), one)
 
@@ -720,7 +731,8 @@
     own_mix.start()
     own_mix.wait()
     widen(0)
-    give(c_fwd, fsend, frecv, ftot, 0)
+    for c in (0, 1):
+        give(c_fwd, fsend, frecv, ftot, 0, c)
     sc_s[...] = jnp.where(causal, dot(qd_s[...], kg_s[...], NT, True), 0.0)
     for i in range(2, 6):
         fetch(i).wait()
@@ -728,23 +740,22 @@
     def half(j, p):
         block = near if j == 0 else near_far
         return remote(
-            part.at[p, :, columns(block)], in1.at[p, j], c_half.send.at[j, p], c_half.recv.at[j, p], (me, near)
+            part.at[p, :, columns(block)], in1.at[p, j], c_half.send, c_half.recv.at[j, p], (me, near)
         )
 
     def cross(p):
-        return remote(out1.at[p], in2.at[p], c_cross.send.at[p], c_cross.recv.at[p], (me, far))
+        return remote(out1.at[p], in2.at[p], c_cross.send, c_cross.recv.at[p], (me, far))
 
     def back(p, slot):
-        return remote(out2.at[p], ret.at[slot], c_back.send.at[p], c_back.recv.at[slot], (p, tp))
+        return remote(out2.at[p], ret.at[slot], c_back.send, c_back.recv, (p, tp))
 
     def expert(m):
         p = peer(m)
 
         @pl.when(m > 0)
         def _():
-            for j in (0, 1):
-                beside(j, p, near).wait_recv()
-                relay(j, p, near_far).wait_recv()
+            arrived(c_beside, p)
+            arrived(c_relay, p)
 
         x = gx[p].reshape(cap, width)
         dy = gdy[p].reshape(cap, width)
@@ -776,11 +787,7 @@
             p = peer(i)
             for j in (0, 1):
                 first(j, p, p).wait_recv()
-
-                @pl.when(i >= close)
-                def _():
-                    across(j, p, tp).start()
-
+                across(j, p, tp).start()
                 beside(j, p, tp).start()
 
         @pl.when((i >= 3) & (i < n_sp + 2))
@@ -790,16 +797,8 @@
         @pl.when((i >= 2) & (i < n_sp + 1))
         def _():
             p = peer(i - 1)
+            arrived(c_across, p)
             for j in (0, 1):
-
-                @pl.when(i - 1 >= close)
-                def _():
-                    across(j, p, far).wait_recv()
-
-                @pl.when(i - 1 < close)
-                def _():
-                    second(j, p, p).wait_recv()
-
                 relay(j, p, far).start()
 
         @pl.when(i >= 4)
@@ -816,12 +815,15 @@
                 back(p, me).start()
 
     expert(0)
-    loop(1, n_sp + 4, step)
+    loop(1, n_sp, step)
+    arrive(0)
+    widen(1)
+    loop(n_sp, n_sp + 2, step)
+    for n in range(1, bits - 1):
+        arrive(n)
+        widen(n + 1)
+    loop(n_sp + 2, n_sp + 4, step)
     ret[me] = out2[me]
-
-    def wait_decay(m):
-        p = flip(m)
-        decay(p, p).wait_recv()
 
     all_x = gx.reshape(n_sp * cap, width)
     all_dy = gdy.reshape(n_sp * cap, width)
@@ -839,19 +841,19 @@
         at = pl.ds(pl.multiple_of(b * tile, tile), tile)
         grad_down[:, at] = dot(hid[...].reshape(n_sp * cap, hid.shape[2]), all_dy[:, at], TN)
 
-    loop(0, width // tile, weight_grad)
-
-    def wait_back(m):
-        p = flip(m)
-        back(p, p).wait_recv()
-
-    loop(1, n_sp, wait_back)
+    def put(i):
+        src = (grad_gate, grad_up, grad_down)[i]
+        return pltpu.make_async_copy(src, (out_gate, out_up, out_down)[i], put_sem.at[i])
+
+    loop(0, width // tile, down_grad)
+    put(2).start()
+    got_all(c_back, ret.at[others])
     acc = dot(comb[...], ret[...].reshape(n_sp * cap, quarter), NN)
     mid[:, columns(tp)] = (acc + dy_in[:, columns(tp)].astype(f32)).astype(bf16)
 
     def spread(k, block, device):
         ref = mid.at[:, columns(block)]
-        return remote(ref, ref, c_share.send.at[k], c_share.recv.at[k], (me, device))
+        return remote(ref, ref, c_share.send, c_share.recv.at[k], (me, device))
 
     def project(block):
         at = pl.ds(pl.multiple_of(block * quarter, quarter), quarter)
@@ -859,11 +861,10 @@
 
     spread(0, tp, far).start()
     spread(1, tp, near).start()
-    loop(1, n_sp, wait_decay)
-    forward_merge(0)
-    give(c_fwd, fsend, frecv, ftot, 1)
-    arrive(0)
-    widen(1)
+    got_all(c_sum, dall.at[others])
+    for c in (0, 1):
+        forward_merge(0, c)
+        give(c_fwd, fsend, frecv, ftot, 1, c)
     head[...] = project(tp)
     spread(1, near, near).wait_recv()
     head[...] += project(near)
@@ -875,59 +876,68 @@
 
     utot[...] = dot(head[...], qd_s[...], TN, True)
     upre[...] = jnp.zeros_like(upre)
-    give(c_rev, usend, urecv, utot, 0)
+    for c in (0, 1):
+        give(c_rev, usend, urecv, utot, 0, c)
 
     def col_first(p, slot):
         at = pl.ds(pl.multiple_of(p * piece, piece), piece)
         mine = pl.ds(pl.multiple_of(tp * rows, rows), rows)
         return remote(
-            mid.at[mine, at], gcols.at[slot, tp], d_first.send.at[p], d_first.recv.at[slot], (p, tp)
+            mid.at[mine, at], gcols.at[slot, tp], d_first.send, d_first.recv, (p, tp)
         )
 
     def col_pass(copies, p, block, device):
         ref = gcols.at[p, block]
-        return remote(ref, ref, copies.send.at[p], copies.recv.at[p], (me, device))
+        return remote(ref, ref, copies.send, copies.recv, (me, device))
 
     def send_cols(m):
         col_first(flip(m), me).start()
 
     loop(1, n_sp, send_cols)
-    for k in range(1, bits - 1):
-        arrive(k)
-        widen(k + 1)
     own_at = pl.ds(pl.multiple_of(me * piece, piece), piece)
     gcols[me] = mid[:, own_at].reshape(n_tp, rows, piece)
     scores_cot = jnp.where(causal, dot(head[...], vv[...].astype(f32), NT, True), 0.0)
     for k in range(1, bits - 1):
-        forward_merge(k)
-        give(c_fwd, fsend, frecv, ftot, k + 1)
+        for c in (0, 1):
+            forward_merge(k, c)
+            give(c_fwd, fsend, frecv, ftot, k + 1, c)
     qc_s[...] = dot(scores_cot, kg_s[...], NN, True)
-    reverse_merge(0)
-    give(c_rev, usend, urecv, utot, 1)
-    loop(0, width // tile, down_grad)
     kc_s[...] = dot(scores_cot, qd_s[...], TN, True)
     gv_s[...] = dot(sc_s[...], head[...], TN, True)
-    for k in range(1, bits):
-        reverse_merge(k)
-        if k < bits - 1:
-            give(c_rev, usend, urecv, utot, k + 1)
-
-        if k == 1:
-            def col_forward(m):
-                p = flip(m)
-                col_first(p, p).wait_recv()
-                col_pass(d_across, p, tp, far).start()
-                col_pass(d_beside, p, tp, near).start()
-
-            loop(1, n_sp, col_forward)
-            def col_relay(m):
-                p = flip(m)
-                col_pass(d_across, p, far, far).wait_recv()
-                col_pass(d_relay, p, far, near).start()
-
-            loop(1, n_sp, col_relay)
-
-    forward_merge(bits - 1)
+
+    def col_forward():
+        got_all(d_first, gcols.at[others, 0])
+
+        def one(m):
+            p = flip(m)
+            col_pass(d_across, p, tp, far).start()
+            col_pass(d_beside, p, tp, near).start()
+
+        loop(1, n_sp, one)
+
+    def col_relay():
+        got_all(d_across, gcols.at[others, 0])
+
+        def one(m):
+            col_pass(d_relay, flip(m), far, near).start()
+
+        loop(1, n_sp, one)
+
+    steps = width // tile
+    for k in range(bits - 1):
+        loop(steps * k // (bits - 1), steps * (k + 1) // (bits - 1), weight_grad)
+        if k == bits - 2:
+            put(0).start()
+            put(1).start()
+            pl.when(me < n_sp // 2)(col_forward)
+        for c in (0, 1):
+            reverse_merge(k, c)
+    pl.when(me >= n_sp // 2)(col_forward)
+    col_relay()
+    for c in (0, 1):
+        reverse_merge(bits - 1, c)
+    for c in (0, 1):
+        forward_merge(bits - 1, c)
     carry, enter = upre[...], fpre[...]
     qc_s[...] += dot(head[...], enter, NN, True)
     cum = cum_s[...]
@@ -946,53 +956,29 @@
 
     arrive(bits - 1)
 
-    def col_finish(m):
-        p = flip(m)
-        col_pass(d_beside, p, near, near).wait_recv()
-        col_pass(d_relay, p, near_far, near).wait_recv()
-
-    loop(1, n_sp, col_finish)
+    got_all(d_beside, gcols.at[others, 0])
+    got_all(d_relay, gcols.at[others, 0])
     grad_proj[...] = dot(
         gcols[...].reshape(n_sp * tok, piece), gmix[...].reshape(n_sp * tok, gmix.shape[2]), TN
     )
 
-    def finish(m):
-        p = peer(m)
-        decay(p, me).wait_send()
-        back(p, me).wait_send()
-        col_first(p, me).wait_send()
-        col_pass(d_across, p, tp, far).wait_send()
-        col_pass(d_beside, p, tp, near).wait_send()
-        col_pass(d_relay, p, far, near).wait_send()
-        for j in (0, 1):
-            first(j, p, me).wait_send()
-
-            @pl.when(m >= close)
-            def _():
-                across(j, p, tp).wait_send()
-
-            @pl.when(m < close)
-            def _():
-                second(j, p, me).wait_send()
-
-            beside(j, p, tp).wait_send()
-            relay(j, p, far).wait_send()
-
-    loop(1, n_sp, finish)
-
-    def finish_return(m):
-        p = flip(m)
-        cross(p).wait_send()
-        for j in (0, 1):
-            half(j, p).wait_send()
-
-    loop(0, n_sp, finish_return)
-    for k in range(bits):
-        hop(c_fwd, fsend, frecv, k).wait_send()
-        hop(c_rev, usend, urecv, k).wait_send()
-    spread(0, tp, far).wait_send()
-    spread(1, tp, near).wait_send()
-    spread(2, far, near).wait_send()
+    def sent(copies, ref):
+        whole(copies, ref).wait_send()
+
+    for copies in (c_first, c_across, c_beside, c_relay):
+        sent(copies, gx.at[others, pl.ds(0, 2)])
+    for copies in (d_first, d_across, d_beside, d_relay):
+        sent(copies, gcols.at[others, 0])
+    sent(c_sum, dall.at[others])
+    sent(c_mix, gmix.at[others])
+    sent(c_fwd, fsend)
+    sent(c_rev, usend)
+    sent(c_half, in1)
+    sent(c_cross, out1)
+    sent(c_back, out2.at[others])
+    sent(c_share, mid.at[:, pl.ds(0, 3 * quarter)])
+    for i in range(3):
+        put(i).wait()
 
 
 def flush_kernel(*refs):
@@ -1035,20 +1021,22 @@
     state = (dv, DK)
     scratch = held + [
         mem((tok, tok), f32), mem((tok, tok), f32), mem((tok, n_sp * cap), bf16),
-        mem((n_sp, 2, share, width), bf16), mem((n_sp, 2, share, width), bf16),
+        mem((n_sp, share, width), bf16), mem((n_sp, share, width), bf16),
         mem((n_sp, n_tp, share, width), bf16), mem((n_sp, n_tp, share, width), bf16),
         mem((n_sp, cap, 2 * units), bf16), mem((n_sp, cap, units), bf16), mem((n_sp, cap, width), bf16),
         mem((n_sp, 2, cap, quarter), bf16),
     ] + [mem((n_sp, cap, quarter), bf16)] * 4 + [
         mem((tok, width), bf16), mem((n_sp,) + args[8].shape, bf16), mem((n_sp, n_tp, tok // n_tp, piece), bf16),
         mem((n_sp, 8, DK), f32),
-    ] + [mem((bits,) + state, bf16)] * 4 + [mem(state, f32)] * 4 + [mem((tok, dv), f32)] + [
+    ] + [mem((bits, 2, dv // 2, DK), bf16)] * 4 + [mem(state, f32)] * 4 + [mem((tok, dv), f32)] + [
         mem((tok, DK), f32)
     ] * 3 + [mem((tok, tok), f32), mem((tok, DK), f32), mem((tok, DK), f32), mem((tok, dv), f32), mem((tok, DK), f32)]
-    scratch += [pltpu.SemaphoreType.DMA((11,)), pltpu.SemaphoreType.DMA]
-    scratch += dma(2, n_sp) * 4 + dma(n_sp)
-    scratch += [pltpu.SemaphoreType.DMA((bits, n_sp // 2)), pltpu.SemaphoreType.DMA((n_sp,))]
-    scratch += dma(bits) + dma(2, n_sp) + dma(n_sp) * 2 + dma(3) + dma(bits) + dma(2, n_sp) + dma(n_sp) * 4
+    scratch += [mem((width, units), f32)] * 2 + [mem((units, width), f32)]
+    scratch += [pltpu.SemaphoreType.DMA((11,)), pltpu.SemaphoreType.DMA, pltpu.SemaphoreType.DMA((3,))]
+    one = pltpu.SemaphoreType.DMA
+    counts = [(2, n_sp)] + [(n_sp,)] * 3 + [(), (n_sp,)] + [(bits, 2), (2, n_sp), (n_sp,), (), (3,), (bits, 2)] + [()] * 4
+    for count in counts:
+        scratch += [one, one(count) if count else one]
     shapes = [
         ((width, units), f32), ((width, units), f32), ((units, width), f32), ((piece, args[8].shape[1]), f32),
         (args[9].shape, bf16), (args[10].shape, bf16), (args[11].shape, bf16), (args[12].shape, f32),
@@ -1057,7 +1045,7 @@
         functools.partial(whole_kernel, n_sp, n_tp),
         out_shape=tuple(pltpu.VMEM(s, t) for s, t in shapes),
         in_specs=[ANY, ANY, VM, VM] + [ANY] * 9,
-        out_specs=(VM,) * 8,
+        out_specs=(ANY,) * 3 + (VM,) * 5,
         scratch_shapes=scratch,
         compiler_params=pltpu.CompilerParams(
             collective_id=3, has_side_effects=True, vmem_limit_bytes=56 * 1024 * 1024

time: 80 us -> 74.2 us (0.927)
  Pallas kernels: 79.2 us -> 73.3 us
    pallas_call x1, Pallas kernels: 76.4 us -> 70.5 us  [whole_plan(): pl.pallas_call(functools.partial(whole_kernel, n_sp, n_tp), out_shape=tup...]
where the time goes in v3:
time: 74.2 us; the launch traced here: 74 us
  Pallas kernels  73.3 us (99%)
    pallas_call x1, Pallas kernels, whole_plan(): pl.pallas_call(functools.partial(whole_kernel, n_sp, n_tp), out_shape=tup...  70.5 us
    pallas_call x1, Pallas kernels, flush(): pl.pallas_call(flush_kernel, out_shape=tuple((jax.ShapeDtypeStruct(a.shap...  2.83 us

profile of v3, /device:TPU:0, one launch (start us, length us, event | category | flops | bytes accessed | tf_op | source)
XLA Modules:
  0.0 74.0 jit_solution(17362793122848129632)
XLA Ops:
  0.6 70.5 %shard_map.188 = (f32[2048,256]{1,0:T(8,128)S(1)}, f32[2048,256]{1,0:T(8,128)S(1)}, f32[256,2048]{1,0:T(8,128)S(1)}, f32[256,256]{1,0:T(8,128)S(1)}, bf16[128,12...) custom-call(bf16[128,2048]{1,0:T(8,128)(2,1)} %refs_0_.1, ...), custom_call_target="tpu_custom_call" | custom-call | tf_op jit(solution)/shard_map/pallas_call | solution.py:1044
  71.2 2.8 %shard_map.189 = (f32[2048,256]{1,0:T(8,128)}, f32[2048,256]{1,0:T(8,128)}, f32[256,2048]{1,0:T(8,128)}, f32[256,256]{1,0:T(8,128)}, bf16[128,128]{1,0:T(8,128)(...) custom-call(f32[2048,256]{1,0:T(8,128)S(1)} %get-tuple-element.24.refs_0_, ...), custom_call_target="tpu_custom_call" | custom-call | tf_op jit(solution)/shard_map/pallas_call | solution.py:997

commit v4 on v3

--- a/solution.py
+++ b/solution.py
@@ -655,6 +655,7 @@
     fpre[...] = jnp.zeros_like(fpre)
 
     piece_rows = ftot.shape[0] // 2
+    is_low, is_high = me < n_sp // 2, me >= n_sp // 2
 
     def hop(copies, held, got, k, c):
         partner = me + (1 << k) * (1 - 2 * lax.rem(me // (1 << k), 2))
@@ -665,7 +666,13 @@
 
     def give(copies, held, got, total, k, c):
         held[k, c] = total[lines(c), :].astype(bf16)
-        hop(copies, held, got, k, c).start()
+        if k < bits - 1:
+            hop(copies, held, got, k, c).start()
+        else:
+
+            @pl.when(is_low if copies is c_fwd else is_high)
+            def _():
+                hop(copies, held, got, k, c).start()
 
     def decay_over(low, high):
         table = dall[:, 0, :]
@@ -688,7 +695,8 @@
         fpre[at, :] = fpre[at, :] + jnp.where(is_upper, decay_over(low, me), 0.0) * got
         mine = jnp.where(is_upper, 1.0, decay_over(low + (1 << k), high + (1 << k)))
         theirs = jnp.where(is_upper, decay_over(low, high), 1.0)
-        ftot[at, :] = mine * ftot[at, :] + theirs * got
+        if k < bits - 1:
+            ftot[at, :] = mine * ftot[at, :] + theirs * got
 
     def reverse_merge(k, c):
         low, high, upper = span(k)
@@ -934,10 +942,17 @@
             reverse_merge(k, c)
     pl.when(me >= n_sp // 2)(col_forward)
     col_relay()
-    for c in (0, 1):
-        reverse_merge(bits - 1, c)
-    for c in (0, 1):
-        forward_merge(bits - 1, c)
+
+    @pl.when(is_low)
+    def _():
+        for c in (0, 1):
+            reverse_merge(bits - 1, c)
+
+    @pl.when(is_high)
+    def _():
+        for c in (0, 1):
+            forward_merge(bits - 1, c)
+
     carry, enter = upre[...], fpre[...]
     qc_s[...] += dot(head[...], enter, NN, True)
     cum = cum_s[...]
@@ -971,8 +986,17 @@
         sent(copies, gcols.at[others, 0])
     sent(c_sum, dall.at[others])
     sent(c_mix, gmix.at[others])
-    sent(c_fwd, fsend)
-    sent(c_rev, usend)
+
+    @pl.when(is_low)
+    def _():
+        sent(c_fwd, fsend)
+        sent(c_rev, usend.at[pl.ds(0, bits - 1)])
+
+    @pl.when(is_high)
+    def _():
+        sent(c_fwd, fsend.at[pl.ds(0, bits - 1)])
+        sent(c_rev, usend)
+
     sent(c_half, in1)
     sent(c_cross, out1)
     sent(c_back, out2.at[others])

time: 74.2 us -> 73.6 us (level)
  no operation moved by 1% of the time
where the time goes in v4:
time: 73.6 us; the launch traced here: 73.4 us
  Pallas kernels  72.8 us (99%)
    pallas_call x1, Pallas kernels, whole_plan(): pl.pallas_call(functools.partial(whole_kernel, n_sp, n_tp), out_shape=tup...  70 us
    pallas_call x1, Pallas kernels, flush(): pl.pallas_call(flush_kernel, out_shape=tuple((jax.ShapeDtypeStruct(a.shap...  2.83 us

profile of v4, /device:TPU:0, one launch (start us, length us, event | category | flops | bytes accessed | tf_op | source)
XLA Modules:
  0.0 73.4 jit_solution(8495517155947904451)
XLA Ops:
  0.6 70.0 %shard_map.188 = (f32[2048,256]{1,0:T(8,128)S(1)}, f32[2048,256]{1,0:T(8,128)S(1)}, f32[256,2048]{1,0:T(8,128)S(1)}, f32[256,256]{1,0:T(8,128)S(1)}, bf16[128,12...) custom-call(bf16[128,2048]{1,0:T(8,128)(2,1)} %refs_0_.1, ...), custom_call_target="tpu_custom_call" | custom-call | tf_op jit(solution)/shard_map/pallas_call | solution.py:1068
  70.6 2.8 %shard_map.189 = (f32[2048,256]{1,0:T(8,128)}, f32[2048,256]{1,0:T(8,128)}, f32[256,2048]{1,0:T(8,128)}, f32[256,256]{1,0:T(8,128)}, bf16[128,128]{1,0:T(8,128)(...) custom-call(f32[2048,256]{1,0:T(8,128)S(1)} %get-tuple-element.24.refs_0_, ...), custom_call_target="tpu_custom_call" | custom-call | tf_op jit(solution)/shard_map/pallas_call | solution.py:1021
